TPU v7x, 128 devices: a whole 4x4x4 slice. The times are simulated.
128 devices in a mesh: ep: 16 (over z, x), tp: 8 (over y, core).
Axes of the slice: x: 4, y: 4, z: 4, core: 2. Of those that a mesh axis runs over, the one named last changes fastest.
Arguments:
- tokens: bfloat16 [16384, 2048], P(('ep', 'tp')), may hold values from -6 to 6
- expert_ids: int32 [16384, 4], P('ep'), may hold values from 0 to 15, all different within a row; in each aligned block of 128 rows (0 to 127, 128 to 255, ...) at most 64 rows name the same one
- gate_values: float32 [16384, 4], P('ep'), may hold values from 0.1 to 1
- norm_gain: float32 [2048], replicated, may hold values from 0.1 to 1.9
- gate_weight: bfloat16 [16, 2048, 1024], P('ep', None, 'tp'), may hold values from -0.125 to 0.125
- up_weight: bfloat16 [16, 2048, 1024], P('ep', None, 'tp'), may hold values from -0.125 to 0.125
- down_weight: bfloat16 [16, 1024, 2048], P('ep', 'tp'), may hold values from -0.1875 to 0.1875
- out_gain: float32 [2048], P('tp'), may hold values from 0.1 to 1.9
Outputs:
- mixed: bfloat16 [16384, 2048], P('ep', 'tp')
Inputs may be any that keep to these rules, and one draw needn't show every extreme that they name: `expert_ids`: each row names 4 different experts of 0 to 15; within the rows of one device (aligned blocks of 128 rows) no expert is named more than 64 times, and in some blocks one expert is named exactly 64 times.
All inputs are finite; a program needn't handle non-finite values.
Results may differ from a plain program's by a relative error of at most 0.0025.
Values may be sent and summed in bfloat16 or wider, within the bound.
No kernel may reach another device: no remote copies, remote signals or barrier semaphores. Data moves between devices by JAX's collectives and lax.ppermute only.
A program may use at most 64 MiB of HBM per device.

v0:
```python
import functools
import jax
import jax.numpy as jnp
from jax import lax
from jax.experimental import pallas as pl
from jax.experimental.pallas import tpu as pltpu
from jax.sharding import PartitionSpec as P

epsilon = 1e-05
clamp_limit = 7.0
sigmoid_alpha = 1.702
f32, bf16 = jnp.float32, jnp.bfloat16


def routing(ids, experts):
    top, tokens = ids.shape
    line = lax.broadcasted_iota(jnp.int32, (experts, tokens), 0)
    named = jnp.zeros((experts, tokens), f32)
    for k in range(top):
        named = named + jnp.where(ids[k : k + 1, :] == line, 1.0, 0.0)
    row = lax.broadcasted_iota(jnp.int32, (tokens, tokens), 0)
    col = lax.broadcasted_iota(jnp.int32, (tokens, tokens), 1)
    before = jnp.where(row < col, 1.0, 0.0).astype(bf16)
    earlier = jnp.dot(named.astype(bf16), before, preferred_element_type=f32)
    return jnp.where(named > 0.5, earlier, -1000.0)


def dispatch_kernel(rank, tokens_ref, ids_ref, gain_ref, out_ref, normed_ref, slot_ref, *, experts, cap):
    tokens = tokens_ref.shape[0]
    group = out_ref.shape[0]

    @pl.when(pl.program_id(0) == 0)
    def _():
        values = tokens_ref[...].astype(f32)
        mean_sq = jnp.mean(values * values, axis=-1, keepdims=True)
        normed_ref[...] = (values * lax.rsqrt(mean_sq + epsilon) * gain_ref[...]).astype(bf16)
        slots = routing(ids_ref[...], experts)
        for i in range(experts // group):
            slot_ref[i] = slots[i * group : (i + 1) * group]

    slots = slot_ref[pl.program_id(0)]
    want = lax.broadcasted_iota(jnp.int32, (cap, tokens), 0).astype(f32)
    chosen = jnp.concatenate(
        [jnp.where(slots[i : i + 1] == want, 1.0, 0.0).astype(bf16) for i in range(group)], axis=0
    )
    picked = jnp.dot(chosen, normed_ref[...], preferred_element_type=f32).astype(bf16)
    for i in range(group):
        out_ref[i] = picked[i * cap : (i + 1) * cap]


def dispatch(rank, tokens, ids, gain, experts, cap):
    rows, width = tokens.shape
    group = 4
    return pl.pallas_call(
        functools.partial(dispatch_kernel, experts=experts, cap=cap),
        out_shape=jax.ShapeDtypeStruct((experts, cap, width), bf16),
        grid_spec=pltpu.PrefetchScalarGridSpec(
            num_scalar_prefetch=1,
            grid=(experts // group,),
            in_specs=[
                pl.BlockSpec((rows, width), lambda e, r: (0, 0)),
                pl.BlockSpec((ids.shape[0], rows), lambda e, r: (0, r[0])),
                pl.BlockSpec((1, width), lambda e, r: (0, 0)),
            ],
            out_specs=pl.BlockSpec((group, cap, width), lambda e, r: (e, 0, 0)),
            scratch_shapes=[
                pltpu.VMEM((rows, width), bf16),
                pltpu.VMEM((experts // group, group, rows), f32),
            ],
        ),
        name="dispatch",
    )(rank, tokens, ids, gain)


def expert_kernel(rows_hbm, *rest, parts):
    gu = rest[:parts]
    dn = rest[parts : 2 * parts]
    out_hbm = rest[2 * parts]
    rows_v, gu_v, dn_v, act_v, out_v, row_sem, gu_sem, dn_sem, out_sem = rest[2 * parts + 1 :]
    hid = dn[0].shape[0]
    total, width = rows_v.shape
    nrow = row_sem.shape[0]
    step = total // nrow
    nout = out_sem.shape[0]
    ocols = width // nout
    row_copies = [
        pltpu.make_async_copy(
            rows_hbm.at[pl.ds(i * step, step)], rows_v.at[pl.ds(i * step, step)], row_sem.at[i]
        )
        for i in range(nrow)
    ]
    gu_copies = [pltpu.make_async_copy(gu[i], gu_v.at[i], gu_sem.at[i]) for i in range(parts)]
    dn_copies = [
        pltpu.make_async_copy(dn[i], dn_v.at[pl.ds(i * hid, hid)], dn_sem.at[i]) for i in range(parts)
    ]
    gu_copies[0].start()
    for c in row_copies:
        c.start()
    gu_copies[1].start()
    for i in range(parts):
        if i + 2 < parts:
            gu_copies[i + 2].start()
        dn_copies[i].start()
        gu_copies[i].wait()
        for m in range(nrow):
            if i == 0:
                row_copies[m].wait()
            span = pl.ds(m * step, step)
            h = jnp.dot(rows_v[span, :], gu_v[i], preferred_element_type=f32)
            g = jnp.minimum(h[:, :hid], clamp_limit)
            u = jnp.clip(h[:, hid:], -clamp_limit, clamp_limit)
            act = g * jax.nn.sigmoid(sigmoid_alpha * g) * (u + 1.0)
            act_v[span, i * hid : (i + 1) * hid] = act.astype(bf16)
    for c in dn_copies:
        c.wait()
    out_copies = []
    for n in range(nout):
        cols = pl.ds(n * ocols, ocols)
        out_v[:, cols] = jnp.dot(act_v[...], dn_v[:, cols], preferred_element_type=f32).astype(bf16)
        c = pltpu.make_async_copy(out_v.at[:, cols], out_hbm.at[:, cols], out_sem.at[n])
        c.start()
        out_copies.append(c)
    for c in out_copies:
        c.wait()


def expert_unit(rows, gu, dn):
    total, width = rows.shape
    parts = len(gu)
    hid = dn[0].shape[0]
    hbm = pl.BlockSpec(memory_space=pl.ANY)
    return pl.pallas_call(
        functools.partial(expert_kernel, parts=parts),
        out_shape=jax.ShapeDtypeStruct((total, width), bf16),
        in_specs=[hbm] * (1 + 2 * parts),
        out_specs=hbm,
        scratch_shapes=[
            pltpu.VMEM((total, width), bf16),
            pltpu.VMEM((parts, width, 2 * hid), bf16),
            pltpu.VMEM((parts * hid, width), bf16),
            pltpu.VMEM((total, parts * hid), bf16),
            pltpu.VMEM((total, width), bf16),
            pltpu.SemaphoreType.DMA((4,)),
            pltpu.SemaphoreType.DMA((parts,)),
            pltpu.SemaphoreType.DMA((parts,)),
            pltpu.SemaphoreType.DMA((4,)),
        ],
        compiler_params=pltpu.CompilerParams(vmem_limit_bytes=56 * 2**20),
        cost_estimate=pl.CostEstimate(
            flops=6 * total * width * parts * hid, bytes_accessed=20 * 2**20, transcendentals=total * parts * hid
        ),
        name="expert_unit",
    )(rows, *gu, *dn)


def combine_kernel(rank, ids_ref, gates_ref, gain_ref, back_hbm, out_ref, back_v, spread_v, acc_v, sem, *, experts, cap):
    top, tokens = ids_ref.shape
    width = back_v.shape[1]
    chunks = sem.shape[0]
    cols = width // chunks
    copies = [
        pltpu.make_async_copy(
            back_hbm.at[:, pl.ds(c * cols, cols)], back_v.at[:, pl.ds(c * cols, cols)], sem.at[c]
        )
        for c in range(chunks)
    ]
    for c in copies:
        c.start()
    ids = ids_ref[...]
    gates = gates_ref[...]
    line = lax.broadcasted_iota(jnp.int32, (experts, tokens), 0)
    weight = jnp.zeros((experts, tokens), f32)
    for k in range(top):
        weight = weight + jnp.where(ids[k : k + 1, :] == line, gates[k : k + 1, :], 0.0)
    filler = jnp.zeros((tokens - 2 * experts, tokens), f32)
    table = jnp.transpose(jnp.concatenate([routing(ids, experts), weight, filler], axis=0))
    col = lax.broadcasted_iota(jnp.int32, (tokens, 2 * cap), 1).astype(f32)
    for e in range(0, experts, 2):
        slot_a, slot_b = table[:, e : e + 1], table[:, e + 1 : e + 2] + cap
        gate_a, gate_b = table[:, experts + e : experts + e + 1], table[:, experts + e + 1 : experts + e + 2]
        spread = jnp.where(col == slot_a, gate_a, 0.0) + jnp.where(col == slot_b, gate_b, 0.0)
        for p in range(3):
            part = spread.astype(bf16)
            spread_v[p * tokens : (p + 1) * tokens, e * cap : (e + 2) * cap] = part
            spread = spread - part.astype(f32)
    total_sq = jnp.zeros((tokens, 1), f32)
    for c in range(chunks):
        copies[c].wait()
        span = pl.ds(c * cols, cols)
        prod = jnp.dot(spread_v[...], back_v[:, span], preferred_element_type=f32)
        combined = prod[:tokens] + prod[tokens : 2 * tokens] + prod[2 * tokens :]
        total_sq = total_sq + jnp.sum(combined * combined, axis=-1, keepdims=True)
        acc_v[:, span] = combined
    scale = lax.rsqrt(total_sq / width + epsilon)
    slices, _, w = out_ref.shape
    for i in range(slices):
        span = pl.ds(i * w, w)
        out_ref[i] = (acc_v[:, span] * scale * gain_ref[:, span]).astype(bf16)


def combine(rank, ids, gates, gain, back, rows, experts, cap, slices):
    width = back.shape[1]
    top = ids.shape[0]
    return pl.pallas_call(
        functools.partial(combine_kernel, experts=experts, cap=cap),
        out_shape=jax.ShapeDtypeStruct((slices, rows, width // slices), bf16),
        grid_spec=pltpu.PrefetchScalarGridSpec(
            num_scalar_prefetch=1,
            grid=(1,),
            in_specs=[
                pl.BlockSpec((top, rows), lambda s, r: (0, r[0])),
                pl.BlockSpec((top, rows), lambda s, r: (0, r[0])),
                pl.BlockSpec((1, width), lambda s, r: (0, 0)),
                pl.BlockSpec(memory_space=pl.ANY),
            ],
            out_specs=pl.BlockSpec((slices, rows, width // slices), lambda s, r: (0, 0, 0)),
            scratch_shapes=[
                pltpu.VMEM((experts * cap, width), bf16),
                pltpu.VMEM((3 * rows, experts * cap), bf16),
                pltpu.VMEM((rows, width), f32),
                pltpu.SemaphoreType.DMA((4,)),
            ],
        ),
        name="combine",
    )(rank, ids, gates, gain, back)


def moved(x, step):
    n = lax.axis_size("tp")
    return lax.ppermute(x, "tp", [(i, step(i)) for i in range(n)])


def local(
    tokens, expert_ids, gate_values, norm_gain, gate_weight, up_weight, down_weight, out_gain
):
    experts = lax.axis_size("ep")
    n_tp = lax.axis_size("tp")
    rows, width = tokens.shape
    cap = rows // 2
    rank = lax.axis_index("tp").reshape(1).astype(jnp.int32)
    ids, gates = expert_ids.T, gate_values.T

    gu_own = jnp.concatenate([gate_weight[0], up_weight[0]], axis=1)
    dn_own = down_weight[0]

    def around(x):
        out = [x]
        for d in (2, n_tp - 2, 4):
            out.append(moved(x, lambda i: (i + d) % n_tp))
        return out

    def across(xs):
        out = []
        for x in xs:
            out.append(moved(x, lambda i: i ^ 1))
        return out

    gu_near = around(gu_own)
    dn_near = around(dn_own)
    gu = gu_near + across(gu_near)
    dn = dn_near + across(dn_near)

    gain_full = lax.all_gather(out_gain, "tp", axis=0, tiled=True)
    outgoing = dispatch(rank, tokens, ids, norm_gain.reshape(1, width), experts, cap)
    arrived = lax.all_to_all(outgoing, "ep", split_axis=0, concat_axis=0, tiled=True)
    result = expert_unit(arrived.reshape(experts * cap, width), gu, dn)
    back = lax.all_to_all(
        result.reshape(experts, cap, width), "ep", split_axis=0, concat_axis=0, tiled=True
    )
    mixed = combine(
        rank, ids, gates, gain_full.reshape(1, width),
        back.reshape(experts * cap, width), rows, experts, cap, n_tp,
    )
    final = lax.all_to_all(mixed, "tp", split_axis=0, concat_axis=0, tiled=True)
    return final.reshape(n_tp * rows, width // n_tp)


def solution(mesh):
    in_specs = (
        P(("ep", "tp"), None),
        P("ep", None),
        P("ep", None),
        P(),
        P("ep", None, "tp"),
        P("ep", None, "tp"),
        P("ep", "tp", None),
        P("tp"),
    )
    out_specs = P("ep", "tp")
    return jax.shard_map(local, mesh=mesh, in_specs=in_specs, out_specs=out_specs, check_vma=False)
```

profile of v0, /device:TPU:1, one launch (start us, length us, event | category | flops | bytes accessed | tf_op | source)
XLA Modules:
  0.0 202.5 jit_solution(4202909245674381926)
XLA Ops:
  0.0 4.5 %dispatch.1 = bf16[16,64,2048]{2,1,0:T(8,128)(2,1)} custom-call(s32[1]{0:T(128)} %bitcast.rank, bf16[128,2048]{1,0:T(8,128)(2,1)} %tokens_ref.1, s32[4,1024]{1,0:T(4,128)} %bitcast.17, f32[1,2048]{1,0:T(1,128)} %bitcast.21), custom_call_target="tpu_custom_call" | custom-call | tf_op jit(solution)/shard_map/dispatch/pallas_call | solution.py:54
  4.5 0.0 copy-start.2
  4.5 8.6 %all-to-all-start = ((bf16[16,64,2048]{2,1,0:T(8,128)(2,1)}), bf16[16,64,2048]{2,1,0:T(8,128)(2,1)}, u32[]{:S(2)}, u32[]{:S(2)}) async-start(bf16[16,64,2048]{2,1,0:T(8,128)(2,1)} %dispatch.1), calls=%async_computation | async-start | bytes 8388608 | tf_op jit(solution)/shard_map/all_to_all | solution.py:265
  13.1 1.4 collective-permute-start.7
  14.5 1.5 collective-permute-start.8
  16.0 1.6 collective-permute-start.9
  17.6 0.0 copy-done.1
  17.6 0.0 copy-done.2
  17.6 0.1 pad_maximum_fusion.rest_0_
  17.7 0.0 copy-start
  17.7 0.5 collective-permute-start
  18.2 2.3 %collective-permute-start.1 = (bf16[2048,256]{1,0:T(8,128)(2,1)S(1)}, bf16[2048,256]{1,0:T(8,128)(2,1)S(1)}, u32[]{:S(2)}, u32[]{:S(2)}) collective-permute-start(bf16[2048,256]{1,0:T(8,128)(2,1)S(1)} %pad_maximum_fusion.rest_0_), channel_id=1, source_target_pairs={{0,6},{1,7},{2,0},{3,1},{4,2},{5,3},{6,4},{7,5},{8,14},{9,15},{10,... | collective-permute-start | bytes 3145736 | tf_op jit(solution)/shard_map/ppermute | solution.py:230
  20.5 6.9 %collective-permute-done.7.rest_9_ = bf16[128,2048]{1,0:T(8,128)(2,1)S(1)} collective-permute-done((bf16[128,2048]{1,0:T(8,128)(2,1)}, bf16[128,2048]{1,0:T(8,128)(2,1)S(1)}, u32[]{:S(2)}, u32[]{:S(2)}) %collective-permute-start.7) | collective-permute-done | bytes 524320 | tf_op jit(solution)/shard_map/ppermute | solution.py:230
  27.4 0.0 copy-start.10
  27.4 1.7 collective-permute-start.2
  29.1 0.0 collective-permute-done.8.rest_10_
  29.1 0.0 copy-start.11
  29.1 14.5 %collective-permute-start.10 = (bf16[128,2048]{1,0:T(8,128)(2,1)}, bf16[128,2048]{1,0:T(8,128)(2,1)S(1)}, u32[]{:S(2)}, u32[]{:S(2)}) collective-permute-start(bf16[128,2048]{1,0:T(8,128)(2,1)} %bitcast.9.rest_8_), channel_id=1, source_target_pairs={{0,1},{1,0},{2,3},{3,2},{4,5},{5,4},{6,7},{7,6},{8,9},{9,8},{10,11... | collective-permute-start | bytes 1572872 | tf_op jit(solution)/shard_map/ppermute | solution.py:230
  43.6 0.0 collective-permute-done.9.rest_11_
  43.6 0.0 copy-start.12
  43.6 0.1 collective-permute-start.3
  43.7 1.6 collective-permute-done.10.rest_12_
  45.4 0.0 copy-start.13
  45.4 0.4 collective-permute-start.11
  45.7 0.4 copy-done.13
  46.2 14.9 %collective-permute-done.rest_1_ = bf16[2048,256]{1,0:T(8,128)(2,1)S(1)} collective-permute-done((bf16[2048,256]{1,0:T(8,128)(2,1)S(1)}, bf16[2048,256]{1,0:T(8,128)(2,1)S(1)}, u32[]{:S(2)}, u32[]{:S(2)}) %collective-permute-start) | collective-permute-done | bytes 1048608 | tf_op jit(solution)/shard_map/ppermute | solution.py:230
  61.1 0.0 copy-start.4
  61.1 1.8 collective-permute-start.4
  62.9 0.0 collective-permute-done.1.rest_2_
  62.9 21.7 %collective-permute-start.5 = (bf16[2048,256]{1,0:T(8,128)(2,1)S(1)}, bf16[2048,256]{1,0:T(8,128)(2,1)S(1)}, u32[]{:S(2)}, u32[]{:S(2)}) collective-permute-start(bf16[2048,256]{1,0:T(8,128)(2,1)S(1)} %collective-permute-done.1.rest_2_), channel_id=1, source_target_pairs={{0,1},{1,0},{2,3},{3,2},{4,5},{5,4},{6,7},{7,6},{8,9},{9,8},{10,11... | collective-permute-start | bytes 3145736 | tf_op jit(solution)/shard_map/ppermute | solution.py:230
  84.6 0.0 collective-permute-done.2.rest_3_
  84.6 1.8 collective-permute-start.6
  86.4 0.0 collective-permute-done.3.rest_4_
  86.4 0.1 collective-permute-start.12
  86.5 0.0 collective-permute-done.11.rest_13_
  86.5 0.4 collective-permute-start.13
  87.0 2.5 %collective-permute-done.12.rest_14_ = bf16[128,2048]{1,0:T(8,128)(2,1)S(1)} collective-permute-done((bf16[128,2048]{1,0:T(8,128)(2,1)S(1)}, bf16[128,2048]{1,0:T(8,128)(2,1)S(1)}, u32[]{:S(2)}, u32[]{:S(2)}) %collective-permute-start.12) | collective-permute-done | bytes 524320 | tf_op jit(solution)/shard_map/ppermute | solution.py:230
  89.5 0.7 collective-permute-done.13.rest_15_
  90.2 0.0 collective-permute-done.4.rest_5_
  90.2 0.0 collective-permute-done.5.rest_6_
  90.2 0.0 copy-done.10
  90.3 0.0 copy-done.11
  90.3 0.0 copy-done.12
  90.3 0.0 copy-done.6
  90.3 0.0 copy-done.7
  90.3 0.0 copy-done.14
  90.3 0.0 copy-done.15
  90.3 0.7 copy-done.16
  91.0 0.4 copy-done.8
  91.4 1.0 copy-done.9
  92.4 0.0 collective-permute-done.6.rest_7_
  92.4 0.0 all-to-all-done
  92.4 0.0 copy-done
  92.4 0.0 copy-done.4
  92.4 0.0 copy-done.5
  92.4 19.1 %expert_unit.1 = bf16[1024,2048]{1,0:T(8,128)(2,1)} custom-call(bf16[1024,2048]{1,0:T(8,128)(2,1)} %bitcast.6.rows_hbm, bf16[2048,256]{1,0:T(8,128)(2,1)} %copy-done, bf16[2048,256]{1,0:T(8,128)(2,1)} %copy-done.4, bf16[2048,256]{1,0:T(8,128)(2,1)} %copy-done.5, bf16[2048,256]{1,0:T(8,128)(2,1)} %copy-done.6, bf16[2048,256]{1,0:T(8,128)(2,1)} %copy-done.7, ...), custom_call_target="tpu_custom_call" | custom-call | flops 12884901888 | bytes 20971520 | tf_op jit(solution)/shard_map/expert_unit/pallas_call | solution.py:132
  111.5 0.0 copy-start.3
  111.5 6.6 %all-to-all-start.1 = ((bf16[16,64,2048]{2,1,0:T(8,128)(2,1)}), bf16[16,64,2048]{2,1,0:T(8,128)(2,1)}, u32[]{:S(2)}, u32[]{:S(2)}) async-start(bf16[16,64,2048]{2,1,0:T(8,128)(2,1)} %bitcast.13), calls=%async_computation.1 | async-start | bytes 8388608 | tf_op jit(solution)/shard_map/all_to_all | solution.py:267
  118.1 0.0 copy-done.3
  118.1 12.4 %all-gather = f32[8,1,256]{2,1,0:T(1,128)} all-gather(f32[1,1,256]{2,1,0:T(1,128)S(1)} %bitcast.22), channel_id=1, replica_groups=mesh['ep'=16,'tp'=8] {'tp'}, dimensions={0}, use_global_device_ids=true | all-gather | bytes 9216 | tf_op jit(solution)/shard_map/all_gather | solution.py:263
  130.5 50.4 %all-to-all-done.1 = bf16[16,64,2048]{2,1,0:T(8,128)(2,1)} async-done(((bf16[16,64,2048]{2,1,0:T(8,128)(2,1)}), bf16[16,64,2048]{2,1,0:T(8,128)(2,1)}, u32[]{:S(2)}, u32[]{:S(2)}) %all-to-all-start.1) | async-done | bytes 4194336 | tf_op jit(solution)/shard_map/all_to_all | solution.py:267
  180.9 5.5 %combine.1 = bf16[8,128,256]{2,1,0:T(8,128)(2,1)} custom-call(s32[1]{0:T(128)} %bitcast.rank, s32[4,1024]{1,0:T(4,128)} %bitcast.18, f32[4,1024]{1,0:T(4,128)} %bitcast.20, f32[1,2048]{1,0:T(1,128)} %bitcast.19, bf16[1024,2048]{1,0:T(8,128)(2,1)} %bitcast.11.back_hbm), custom_call_target="tpu_custom_call" | custom-call | tf_op jit(solution)/shard_map/combine/pallas_call | solution.py:204
  186.4 15.4 %all_to_all.15 = bf16[8,128,256]{2,1,0:T(8,128)(2,1)S(1)} all-to-all(bf16[8,128,256]{2,1,0:T(8,128)(2,1)} %combine.1), channel_id=1, replica_groups=mesh['ep'=16,'tp'=8] {'tp'}, dimensions={0} | all-to-all | bytes 1048576 | tf_op jit(solution)/shard_map/all_to_all | solution.py:274
  201.7 0.8 copy.10
  (9 shorter events, 0.0 us)
Async XLA Ops:
  4.5 13.1 %copy-start.1 = (bf16[1,2048,128]{2,1,0:T(8,128)(2,1)S(1)}, bf16[1,2048,128]{2,1,0:T(8,128)(2,1)}, u32[]{:S(2)}) copy-start(bf16[1,2048,128]{2,1,0:T(8,128)(2,1)} %param.13) | copy-start | bytes 1572868
  4.5 13.1 %copy-start.2 = (bf16[1,2048,128]{2,1,0:T(8,128)(2,1)S(1)}, bf16[1,2048,128]{2,1,0:T(8,128)(2,1)}, u32[]{:S(2)}) copy-start(bf16[1,2048,128]{2,1,0:T(8,128)(2,1)} %param.12) | copy-start | bytes 1572868
  4.5 87.8 %all-to-all-start = ((bf16[16,64,2048]{2,1,0:T(8,128)(2,1)}), bf16[16,64,2048]{2,1,0:T(8,128)(2,1)}, u32[]{:S(2)}, u32[]{:S(2)}) async-start(bf16[16,64,2048]{2,1,0:T(8,128)(2,1)} %dispatch.1), calls=%async_computation | async-start | bytes 8388608 | tf_op jit(solution)/shard_map/all_to_all | solution.py:265
  13.1 14.3 %collective-permute-start.7 = (bf16[128,2048]{1,0:T(8,128)(2,1)}, bf16[128,2048]{1,0:T(8,128)(2,1)S(1)}, u32[]{:S(2)}, u32[]{:S(2)}) collective-permute-start(bf16[128,2048]{1,0:T(8,128)(2,1)} %bitcast.9.rest_8_), channel_id=1, source_target_pairs={{0,2},{1,3},{2,4},{3,5},{4,6},{5,7},{6,0},{7,1},{8,10},{9,11},{10,... | collective-permute-start | bytes 1572872 | tf_op jit(solution)/shard_map/ppermute | solution.py:230
  14.5 14.6 %collective-permute-start.8 = (bf16[128,2048]{1,0:T(8,128)(2,1)}, bf16[128,2048]{1,0:T(8,128)(2,1)S(1)}, u32[]{:S(2)}, u32[]{:S(2)}) collective-permute-start(bf16[128,2048]{1,0:T(8,128)(2,1)} %bitcast.9.rest_8_), channel_id=1, source_target_pairs={{0,6},{1,7},{2,0},{3,1},{4,2},{5,3},{6,4},{7,5},{8,14},{9,15},{10,... | collective-permute-start | bytes 1572872 | tf_op jit(solution)/shard_map/ppermute | solution.py:230
  16.0 27.6 %collective-permute-start.9 = (bf16[128,2048]{1,0:T(8,128)(2,1)}, bf16[128,2048]{1,0:T(8,128)(2,1)S(1)}, u32[]{:S(2)}, u32[]{:S(2)}) collective-permute-start(bf16[128,2048]{1,0:T(8,128)(2,1)} %bitcast.9.rest_8_), channel_id=1, source_target_pairs={{0,4},{1,5},{2,6},{3,7},{4,0},{5,1},{6,2},{7,3},{8,12},{9,13},{10,... | collective-permute-start | bytes 1572872 | tf_op jit(solution)/shard_map/ppermute | solution.py:230
  17.7 74.7 %copy-start = (bf16[2048,256]{1,0:T(8,128)(2,1)}, bf16[2048,256]{1,0:T(8,128)(2,1)S(1)}, u32[]{:S(2)}) copy-start(bf16[2048,256]{1,0:T(8,128)(2,1)S(1)} %pad_maximum_fusion.rest_0_) | copy-start | bytes 3145732
  17.7 43.4 %collective-permute-start = (bf16[2048,256]{1,0:T(8,128)(2,1)S(1)}, bf16[2048,256]{1,0:T(8,128)(2,1)S(1)}, u32[]{:S(2)}, u32[]{:S(2)}) collective-permute-start(bf16[2048,256]{1,0:T(8,128)(2,1)S(1)} %pad_maximum_fusion.rest_0_), channel_id=1, source_target_pairs={{0,2},{1,3},{2,4},{3,5},{4,6},{5,7},{6,0},{7,1},{8,10},{9,11},{10,... | collective-permute-start | bytes 3145736 | tf_op jit(solution)/shard_map/ppermute | solution.py:230
  18.2 44.7 %collective-permute-start.1 = (bf16[2048,256]{1,0:T(8,128)(2,1)S(1)}, bf16[2048,256]{1,0:T(8,128)(2,1)S(1)}, u32[]{:S(2)}, u32[]{:S(2)}) collective-permute-start(bf16[2048,256]{1,0:T(8,128)(2,1)S(1)} %pad_maximum_fusion.rest_0_), channel_id=1, source_target_pairs={{0,6},{1,7},{2,0},{3,1},{4,2},{5,3},{6,4},{7,5},{8,14},{9,15},{10,... | collective-permute-start | bytes 3145736 | tf_op jit(solution)/shard_map/ppermute | solution.py:230
  27.4 62.8 %copy-start.10 = (bf16[128,2048]{1,0:T(8,128)(2,1)}, bf16[128,2048]{1,0:T(8,128)(2,1)S(1)}, u32[]{:S(2)}) copy-start(bf16[128,2048]{1,0:T(8,128)(2,1)S(1)} %collective-permute-done.7.rest_9_) | copy-start | bytes 1572868
  27.4 57.2 %collective-permute-start.2 = (bf16[2048,256]{1,0:T(8,128)(2,1)S(1)}, bf16[2048,256]{1,0:T(8,128)(2,1)S(1)}, u32[]{:S(2)}, u32[]{:S(2)}) collective-permute-start(bf16[2048,256]{1,0:T(8,128)(2,1)S(1)} %pad_maximum_fusion.rest_0_), channel_id=1, source_target_pairs={{0,4},{1,5},{2,6},{3,7},{4,0},{5,1},{6,2},{7,3},{8,12},{9,13},{10,... | collective-permute-start | bytes 3145736 | tf_op jit(solution)/shard_map/ppermute | solution.py:230
  29.1 61.2 %copy-start.11 = (bf16[128,2048]{1,0:T(8,128)(2,1)}, bf16[128,2048]{1,0:T(8,128)(2,1)S(1)}, u32[]{:S(2)}) copy-start(bf16[128,2048]{1,0:T(8,128)(2,1)S(1)} %collective-permute-done.8.rest_10_) | copy-start | bytes 1572868
  29.1 16.3 %collective-permute-start.10 = (bf16[128,2048]{1,0:T(8,128)(2,1)}, bf16[128,2048]{1,0:T(8,128)(2,1)S(1)}, u32[]{:S(2)}, u32[]{:S(2)}) collective-permute-start(bf16[128,2048]{1,0:T(8,128)(2,1)} %bitcast.9.rest_8_), channel_id=1, source_target_pairs={{0,1},{1,0},{2,3},{3,2},{4,5},{5,4},{6,7},{7,6},{8,9},{9,8},{10,11... | collective-permute-start | bytes 1572872 | tf_op jit(solution)/shard_map/ppermute | solution.py:230
  43.6 46.6 %copy-start.12 = (bf16[128,2048]{1,0:T(8,128)(2,1)}, bf16[128,2048]{1,0:T(8,128)(2,1)S(1)}, u32[]{:S(2)}) copy-start(bf16[128,2048]{1,0:T(8,128)(2,1)S(1)} %collective-permute-done.9.rest_11_) | copy-start | bytes 1572868
  43.6 42.8 %collective-permute-start.3 = (bf16[2048,256]{1,0:T(8,128)(2,1)S(1)}, bf16[2048,256]{1,0:T(8,128)(2,1)S(1)}, u32[]{:S(2)}, u32[]{:S(2)}) collective-permute-start(bf16[2048,256]{1,0:T(8,128)(2,1)S(1)} %pad_maximum_fusion.rest_0_), channel_id=1, source_target_pairs={{0,1},{1,0},{2,3},{3,2},{4,5},{5,4},{6,7},{7,6},{8,9},{9,8},{10,11... | collective-permute-start | bytes 3145736 | tf_op jit(solution)/shard_map/ppermute | solution.py:230
  45.4 0.8 copy-start.13
  45.4 41.2 %collective-permute-start.11 = (bf16[128,2048]{1,0:T(8,128)(2,1)S(1)}, bf16[128,2048]{1,0:T(8,128)(2,1)S(1)}, u32[]{:S(2)}, u32[]{:S(2)}) collective-permute-start(bf16[128,2048]{1,0:T(8,128)(2,1)S(1)} %collective-permute-done.7.rest_9_), channel_id=1, source_target_pairs={{0,1},{1,0},{2,3},{3,2},{4,5},{5,4},{6,7},{7,6},{8,9},{9,8},{10,11... | collective-permute-start | bytes 1572872 | tf_op jit(solution)/shard_map/ppermute | solution.py:230
  61.1 31.3 %copy-start.4 = (bf16[2048,256]{1,0:T(8,128)(2,1)}, bf16[2048,256]{1,0:T(8,128)(2,1)S(1)}, u32[]{:S(2)}) copy-start(bf16[2048,256]{1,0:T(8,128)(2,1)S(1)} %collective-permute-done.rest_1_) | copy-start | bytes 3145732
  61.1 29.1 %collective-permute-start.4 = (bf16[2048,256]{1,0:T(8,128)(2,1)S(1)}, bf16[2048,256]{1,0:T(8,128)(2,1)S(1)}, u32[]{:S(2)}, u32[]{:S(2)}) collective-permute-start(bf16[2048,256]{1,0:T(8,128)(2,1)S(1)} %collective-permute-done.rest_1_), channel_id=1, source_target_pairs={{0,1},{1,0},{2,3},{3,2},{4,5},{5,4},{6,7},{7,6},{8,9},{9,8},{10,11... | collective-permute-start | bytes 3145736 | tf_op jit(solution)/shard_map/ppermute | solution.py:230
  62.9 29.5 %copy-start.5 = (bf16[2048,256]{1,0:T(8,128)(2,1)}, bf16[2048,256]{1,0:T(8,128)(2,1)S(1)}, u32[]{:S(2)}) copy-start(bf16[2048,256]{1,0:T(8,128)(2,1)S(1)} %collective-permute-done.1.rest_2_) | copy-start | bytes 3145732
  62.9 27.3 %collective-permute-start.5 = (bf16[2048,256]{1,0:T(8,128)(2,1)S(1)}, bf16[2048,256]{1,0:T(8,128)(2,1)S(1)}, u32[]{:S(2)}, u32[]{:S(2)}) collective-permute-start(bf16[2048,256]{1,0:T(8,128)(2,1)S(1)} %collective-permute-done.1.rest_2_), channel_id=1, source_target_pairs={{0,1},{1,0},{2,3},{3,2},{4,5},{5,4},{6,7},{7,6},{8,9},{9,8},{10,11... | collective-permute-start | bytes 3145736 | tf_op jit(solution)/shard_map/ppermute | solution.py:230
  84.6 5.6 %copy-start.6 = (bf16[2048,256]{1,0:T(8,128)(2,1)}, bf16[2048,256]{1,0:T(8,128)(2,1)S(1)}, u32[]{:S(2)}) copy-start(bf16[2048,256]{1,0:T(8,128)(2,1)S(1)} %collective-permute-done.2.rest_3_) | copy-start | bytes 3145732
  84.6 7.7 %collective-permute-start.6 = (bf16[2048,256]{1,0:T(8,128)(2,1)S(1)}, bf16[2048,256]{1,0:T(8,128)(2,1)}, u32[]{:S(2)}, u32[]{:S(2)}) collective-permute-start(bf16[2048,256]{1,0:T(8,128)(2,1)S(1)} %collective-permute-done.2.rest_3_), channel_id=1, source_target_pairs={{0,1},{1,0},{2,3},{3,2},{4,5},{5,4},{6,7},{7,6},{8,9},{9,8},{10,11... | collective-permute-start | bytes 3145736 | tf_op jit(solution)/shard_map/ppermute | solution.py:230
  86.4 3.8 %copy-start.7 = (bf16[2048,256]{1,0:T(8,128)(2,1)}, bf16[2048,256]{1,0:T(8,128)(2,1)S(1)}, u32[]{:S(2)}) copy-start(bf16[2048,256]{1,0:T(8,128)(2,1)S(1)} %collective-permute-done.3.rest_4_) | copy-start | bytes 3145732
  86.4 3.0 %collective-permute-start.12 = (bf16[128,2048]{1,0:T(8,128)(2,1)S(1)}, bf16[128,2048]{1,0:T(8,128)(2,1)S(1)}, u32[]{:S(2)}, u32[]{:S(2)}) collective-permute-start(bf16[128,2048]{1,0:T(8,128)(2,1)S(1)} %collective-permute-done.8.rest_10_), channel_id=1, source_target_pairs={{0,1},{1,0},{2,3},{3,2},{4,5},{5,4},{6,7},{7,6},{8,9},{9,8},{10,11... | collective-permute-start | bytes 1572872 | tf_op jit(solution)/shard_map/ppermute | solution.py:230
  86.5 3.8 %copy-start.14 = (bf16[128,2048]{1,0:T(8,128)(2,1)}, bf16[128,2048]{1,0:T(8,128)(2,1)S(1)}, u32[]{:S(2)}) copy-start(bf16[128,2048]{1,0:T(8,128)(2,1)S(1)} %collective-permute-done.11.rest_13_) | copy-start | bytes 1572868
  86.5 3.7 %collective-permute-start.13 = (bf16[128,2048]{1,0:T(8,128)(2,1)S(1)}, bf16[128,2048]{1,0:T(8,128)(2,1)S(1)}, u32[]{:S(2)}, u32[]{:S(2)}) collective-permute-start(bf16[128,2048]{1,0:T(8,128)(2,1)S(1)} %collective-permute-done.9.rest_11_), channel_id=1, source_target_pairs={{0,1},{1,0},{2,3},{3,2},{4,5},{5,4},{6,7},{7,6},{8,9},{9,8},{10,11... | collective-permute-start | bytes 1572872 | tf_op jit(solution)/shard_map/ppermute | solution.py:230
  89.5 0.8 copy-start.15
  90.2 0.8 copy-start.16
  90.2 1.1 copy-start.8
  91.4 1.0 copy-start.9
  111.5 6.6 %copy-start.3 = (f32[256]{0:T(256)S(1)}, f32[256]{0:T(256)}, u32[]{:S(2)}) copy-start(f32[256]{0:T(256)} %param.15) | copy-start | bytes 3076
  111.5 69.4 %all-to-all-start.1 = ((bf16[16,64,2048]{2,1,0:T(8,128)(2,1)}), bf16[16,64,2048]{2,1,0:T(8,128)(2,1)}, u32[]{:S(2)}, u32[]{:S(2)}) async-start(bf16[16,64,2048]{2,1,0:T(8,128)(2,1)} %bitcast.13), calls=%async_computation.1 | async-start | bytes 8388608 | tf_op jit(solution)/shard_map/all_to_all | solution.py:267
where the time goes:
time: 203 us
  waiting for transfers between devices  77.2 us (38%)
  starting transfers between devices  64.9 us (32%)
  Pallas kernels  29.1 us (14%)
  blocking collectives  27.7 us (14%)
  local copies, waits for them, and re-layouts  3.32 us (2%)
    all_to_all x1, waiting for transfers between devices, local(): lax.all_to_all(result.reshape(experts, cap, width), 'ep', split_axis=0, c...  50.4 us
    ppermute x14, starting transfers between devices, moved(): return lax.ppermute(x, 'tp', [(i, step(i)) for i in range(n)])  49.7 us
    ppermute x14, waiting for transfers between devices, moved(): return lax.ppermute(x, 'tp', [(i, step(i)) for i in range(n)])  26.8 us
    pallas_call x1, Pallas kernels, expert_unit(): pl.pallas_call(functools.partial(expert_kernel, parts=parts), out_shape=j...  19.1 us
    all_to_all x1, blocking collectives, local(): final = lax.all_to_all(mixed, 'tp', split_axis=0, concat_axis=0, tiled=True)  15.4 us
    all_gather x1, blocking collectives, local(): gain_full = lax.all_gather(out_gain, 'tp', axis=0, tiled=True)  12.4 us
    all_to_all x1, starting transfers between devices, local(): lax.all_to_all(outgoing, 'ep', split_axis=0, concat_axis=0, tiled=True)  8.6 us
    all_to_all x1, starting transfers between devices, local(): lax.all_to_all(result.reshape(experts, cap, width), 'ep', split_axis=0, c...  6.6 us
  transfers between devices with their start and end apart: 16, of which 6 were waited for; matrix products, arithmetic and copies ran while one was open for 0% of the time, Pallas kernels for 0%

commit v1 on v0

v1 whole, which is shorter than its diff:
```python
import functools
import jax
import jax.numpy as jnp
from jax import lax
from jax.experimental import pallas as pl
from jax.experimental.pallas import tpu as pltpu
from jax.sharding import PartitionSpec as P

epsilon = 1e-05
clamp_limit = 7.0
sigmoid_alpha = 1.702
f32, bf16 = jnp.float32, jnp.bfloat16


def SPLIT(cap):
    return (cap,)


def routing(ids, experts):
    top, tokens = ids.shape
    line = lax.broadcasted_iota(jnp.int32, (experts, tokens), 0)
    named = jnp.zeros((experts, tokens), f32)
    for k in range(top):
        named = named + jnp.where(ids[k : k + 1, :] == line, 1.0, 0.0)
    row = lax.broadcasted_iota(jnp.int32, (tokens, tokens), 0)
    col = lax.broadcasted_iota(jnp.int32, (tokens, tokens), 1)
    before = jnp.where(row < col, 1.0, 0.0).astype(bf16)
    earlier = jnp.dot(named.astype(bf16), before, preferred_element_type=f32)
    return jnp.where(named > 0.5, earlier, -1000.0)


def dispatch_kernel(rank, tokens_ref, ids_ref, gain_ref, *rest, experts, cap):
    outs, (normed_ref, slot_ref) = rest[:-2], rest[-2:]
    tokens = tokens_ref.shape[0]
    group = outs[0].shape[0]

    @pl.when(pl.program_id(0) == 0)
    def _():
        values = tokens_ref[...].astype(f32)
        mean_sq = jnp.mean(values * values, axis=-1, keepdims=True)
        normed_ref[...] = (values * lax.rsqrt(mean_sq + epsilon) * gain_ref[...]).astype(bf16)
        slots = routing(ids_ref[...], experts)
        for i in range(experts // group):
            slot_ref[i] = slots[i * group : (i + 1) * group]

    slots = slot_ref[pl.program_id(0)]
    want = lax.broadcasted_iota(jnp.int32, (cap, tokens), 0).astype(f32)
    chosen = jnp.concatenate(
        [jnp.where(slots[i : i + 1] == want, 1.0, 0.0).astype(bf16) for i in range(group)], axis=0
    )
    picked = jnp.dot(chosen, normed_ref[...], preferred_element_type=f32).astype(bf16)
    for i in range(group):
        at = i * cap
        for out in outs:
            out[i] = picked[at : at + out.shape[1]]
            at += out.shape[1]


def dispatch(rank, tokens, ids, gain, experts, split):
    rows, width = tokens.shape
    group = 4
    return pl.pallas_call(
        functools.partial(dispatch_kernel, experts=experts, cap=sum(split)),
        out_shape=[jax.ShapeDtypeStruct((experts, n, width), bf16) for n in split],
        grid_spec=pltpu.PrefetchScalarGridSpec(
            num_scalar_prefetch=1,
            grid=(experts // group,),
            in_specs=[
                pl.BlockSpec((rows, width), lambda e, r: (0, 0)),
                pl.BlockSpec((ids.shape[0], rows), lambda e, r: (0, r[0])),
                pl.BlockSpec((1, width), lambda e, r: (0, 0)),
            ],
            out_specs=[pl.BlockSpec((group, n, width), lambda e, r: (e, 0, 0)) for n in split],
            scratch_shapes=[
                pltpu.VMEM((rows, width), bf16),
                pltpu.VMEM((experts // group, group, rows), f32),
            ],
        ),
        name="dispatch",
    )(rank, tokens, ids, gain)


def expert_kernel(rows_hbm, *rest, gu_parts, dn_parts):
    gu = rest[: len(gu_parts)]
    dn = rest[len(gu_parts) : len(gu_parts) + len(dn_parts)]
    out_hbm, rows_v, gu_v, dn_v, act_v, out_v, row_sem, gu_sem, dn_sem, out_sem = rest[len(gu_parts) + len(dn_parts) :]
    parts = gu_v.shape[0]
    hid = gu_v.shape[2] // 2
    total, width = rows_v.shape
    nrow = row_sem.shape[0]
    step = total // nrow
    nout = out_sem.shape[0]
    ocols = width // nout

    row_copies = [
        pltpu.make_async_copy(
            rows_hbm.at[pl.ds(i * step, step)], rows_v.at[pl.ds(i * step, step)], row_sem.at[i]
        )
        for i in range(nrow)
    ]
    gu_copies = [[] for _ in range(parts)]
    for j, (i, at, size) in enumerate(gu_parts):
        gu_copies[i].append(
            pltpu.make_async_copy(gu[j], gu_v.at[i, pl.ds(at, size)], gu_sem.at[j])
        )
    dn_copies = [[] for _ in range(parts)]
    for j, (i, at, size) in enumerate(dn_parts):
        dn_copies[i].append(
            pltpu.make_async_copy(dn[j], dn_v.at[pl.ds(i * hid + at, size)], dn_sem.at[j])
        )
    for c in gu_copies[0] + row_copies + gu_copies[1]:
        c.start()
    for i in range(parts):
        for c in (gu_copies[i + 2] if i + 2 < parts else []) + dn_copies[i]:
            c.start()
        for c in gu_copies[i]:
            c.wait()
        for m in range(nrow):
            if i == 0:
                row_copies[m].wait()
            span = pl.ds(m * step, step)
            h = jnp.dot(rows_v[span, :], gu_v[i], preferred_element_type=f32)
            g = jnp.minimum(h[:, :hid], clamp_limit)
            u = jnp.clip(h[:, hid:], -clamp_limit, clamp_limit)
            act = g * jax.nn.sigmoid(sigmoid_alpha * g) * (u + 1.0)
            act_v[span, i * hid : (i + 1) * hid] = act.astype(bf16)
    for cs in dn_copies:
        for c in cs:
            c.wait()
    out_copies = []
    for n in range(nout):
        cols = pl.ds(n * ocols, ocols)
        out_v[:, cols] = jnp.dot(act_v[...], dn_v[:, cols], preferred_element_type=f32).astype(bf16)
        c = pltpu.make_async_copy(out_v.at[:, cols], out_hbm.at[:, cols], out_sem.at[n])
        c.start()
        out_copies.append(c)
    for c in out_copies:
        c.wait()


def expert_unit(rows, gu, dn, parts, hid):
    total, width = rows.shape
    hbm = pl.BlockSpec(memory_space=pl.ANY)
    return pl.pallas_call(
        functools.partial(
            expert_kernel,
            gu_parts=tuple((i, at, x.shape[0]) for i, at, x in gu),
            dn_parts=tuple((i, at, x.shape[0]) for i, at, x in dn),
        ),
        out_shape=jax.ShapeDtypeStruct((total, width), bf16),
        in_specs=[hbm] * (1 + len(gu) + len(dn)),
        out_specs=hbm,
        scratch_shapes=[
            pltpu.VMEM((total, width), bf16),
            pltpu.VMEM((parts, width, 2 * hid), bf16),
            pltpu.VMEM((parts * hid, width), bf16),
            pltpu.VMEM((total, parts * hid), bf16),
            pltpu.VMEM((total, width), bf16),
            pltpu.SemaphoreType.DMA((total // 256,)),
            pltpu.SemaphoreType.DMA((len(gu),)),
            pltpu.SemaphoreType.DMA((len(dn),)),
            pltpu.SemaphoreType.DMA((4,)),
        ],
        compiler_params=pltpu.CompilerParams(vmem_limit_bytes=48 * 2**20),
        cost_estimate=pl.CostEstimate(
            flops=6 * total * width * parts * hid, bytes_accessed=20 * 2**20, transcendentals=total * parts * hid
        ),
        name="expert_unit",
    )(rows, *[x for _, _, x in gu], *[x for _, _, x in dn])


def combine_kernel(rank, ids_ref, gates_ref, gain_ref, *rest, experts, split):
    backs = rest[: len(split)]
    out_ref, back_v, spread_v, acc_v, sem = rest[len(split) :]
    top, tokens = ids_ref.shape
    width = back_v.shape[1]
    chunks = sem.shape[1]
    cols = width // chunks
    copies = [[] for _ in range(chunks)]
    at = 0
    for j, back in enumerate(backs):
        size = back.shape[0]
        for c in range(chunks):
            span = pl.ds(c * cols, cols)
            copies[c].append(
                pltpu.make_async_copy(back.at[:, span], back_v.at[pl.ds(at, size), span], sem.at[j, c])
            )
        at += size
    for cs in copies:
        for c in cs:
            c.start()
    ids = ids_ref[...]
    gates = gates_ref[...]
    line = lax.broadcasted_iota(jnp.int32, (experts, tokens), 0)
    weight = jnp.zeros((experts, tokens), f32)
    for k in range(top):
        weight = weight + jnp.where(ids[k : k + 1, :] == line, gates[k : k + 1, :], 0.0)
    filler = jnp.zeros((tokens - 2 * experts, tokens), f32)
    table = jnp.transpose(jnp.concatenate([routing(ids, experts), weight, filler], axis=0))
    lanes = 128
    lane = lax.broadcasted_iota(jnp.int32, (tokens, lanes), 1)
    base, first = 0, 0
    for n in split:
        per = lanes // n
        owner = lane // n
        col = (lane % n + first).astype(f32)
        for e in range(0, experts, per):
            spread = jnp.zeros((tokens, lanes), f32)
            for q in range(per):
                hit = (owner == q) & (col == table[:, e + q : e + q + 1])
                spread = jnp.where(hit, table[:, experts + e + q : experts + e + q + 1], spread)
            for p in range(3):
                part = spread.astype(bf16)
                spread_v[p * tokens : (p + 1) * tokens, base : base + lanes] = part
                spread = spread - part.astype(f32)
            base += lanes
        first += n
    total_sq = jnp.zeros((tokens, 1), f32)
    for c in range(chunks):
        for copy in copies[c]:
            copy.wait()
        span = pl.ds(c * cols, cols)
        prod = jnp.dot(spread_v[...], back_v[:, span], preferred_element_type=f32)
        combined = prod[:tokens] + prod[tokens : 2 * tokens] + prod[2 * tokens :]
        total_sq = total_sq + jnp.sum(combined * combined, axis=-1, keepdims=True)
        acc_v[:, span] = combined
    scale = lax.rsqrt(total_sq / width + epsilon)
    slices, _, w = out_ref.shape
    for i in range(slices):
        span = pl.ds(i * w, w)
        out_ref[i] = (acc_v[:, span] * scale * gain_ref[:, span]).astype(bf16)


def combine(rank, ids, gates, gain, backs, rows, experts, split, slices):
    width = backs[0].shape[1]
    top = ids.shape[0]
    return pl.pallas_call(
        functools.partial(combine_kernel, experts=experts, split=split),
        out_shape=jax.ShapeDtypeStruct((slices, rows, width // slices), bf16),
        grid_spec=pltpu.PrefetchScalarGridSpec(
            num_scalar_prefetch=1,
            grid=(1,),
            in_specs=[
                pl.BlockSpec((top, rows), lambda s, r: (0, r[0])),
                pl.BlockSpec((top, rows), lambda s, r: (0, r[0])),
                pl.BlockSpec((1, width), lambda s, r: (0, 0)),
            ]
            + [pl.BlockSpec(memory_space=pl.ANY)] * len(split),
            out_specs=pl.BlockSpec((slices, rows, width // slices), lambda s, r: (0, 0, 0)),
            scratch_shapes=[
                pltpu.VMEM((experts * sum(split), width), bf16),
                pltpu.VMEM((3 * rows, experts * sum(split)), bf16),
                pltpu.VMEM((rows, width), f32),
                pltpu.SemaphoreType.DMA((len(split), 4)),
            ],
        ),
        name="combine",
    )(rank, ids, gates, gain, *backs)


def moved(x, step):
    n = lax.axis_size("tp")
    return lax.ppermute(x, "tp", [(i, step(i)) for i in range(n)])


def local(
    tokens, expert_ids, gate_values, norm_gain, gate_weight, up_weight, down_weight, out_gain
):
    experts = lax.axis_size("ep")
    n_tp = lax.axis_size("tp")
    rows, width = tokens.shape
    cap = rows // 2
    rank = lax.axis_index("tp").reshape(1).astype(jnp.int32)
    ids, gates = expert_ids.T, gate_values.T

    gu_own = jnp.concatenate([gate_weight[0], up_weight[0]], axis=1)
    dn_own = down_weight[0]

    def spread_out(x):
        up, down, other = (lambda i: (i + 2) % n_tp), (lambda i: (i - 2) % n_tp), (lambda i: i ^ 1)
        half = x.shape[0] // 2
        p = moved(x, up)
        m = moved(x, down)
        lo = moved(p[:half], up)
        hi = moved(m[half:], down)
        near = [(0, 0, x), (2, 0, p), (4, 0, m), (6, 0, lo), (6, half, hi)]
        far = [(i + 1, at, moved(a, other)) for i, at, a in near]
        return sorted(near + far, key=lambda entry: entry[:2])

    gu = spread_out(gu_own)
    dn = spread_out(dn_own)

    gain_full = lax.all_gather(out_gain, "tp", axis=0, tiled=True)
    split = SPLIT(cap)
    outgoing = dispatch(rank, tokens, ids, norm_gain.reshape(1, width), experts, split)
    backs = []
    for x in outgoing:
        arrived = lax.all_to_all(x, "ep", split_axis=0, concat_axis=0, tiled=True)
        result = expert_unit(arrived.reshape(-1, width), gu, dn, n_tp, down_weight.shape[1])
        back = lax.all_to_all(
            result.reshape(x.shape), "ep", split_axis=0, concat_axis=0, tiled=True
        )
        backs.append(back.reshape(-1, width))
    mixed = combine(
        rank, ids, gates, gain_full.reshape(1, width), backs, rows, experts, split, n_tp,
    )
    final = lax.all_to_all(mixed, "tp", split_axis=0, concat_axis=0, tiled=True)
    return final.reshape(n_tp * rows, width // n_tp)


def solution(mesh):
    in_specs = (
        P(("ep", "tp"), None),
        P("ep", None),
        P("ep", None),
        P(),
        P("ep", None, "tp"),
        P("ep", None, "tp"),
        P("ep", "tp", None),
        P("tp"),
    )
    out_specs = P("ep", "tp")
    return jax.shard_map(local, mesh=mesh, in_specs=in_specs, out_specs=out_specs, check_vma=False)
```

time: 203 us -> 201 us (level)
  starting transfers between devices: 64.9 us -> 35.7 us
  waiting for transfers between devices: 77.2 us -> 94.9 us
  local copies, waits for them, and re-layouts: 3.32 us -> 12.8 us
    ppermute x14 -> x18, starting transfers between devices: 49.7 us -> 20.5 us  [moved(): return lax.ppermute(x, 'tp', [(i, step(i)) for i in range(n)])]
    ppermute x14 -> x18, waiting for transfers between devices: 26.8 us -> 43.6 us  [moved(): return lax.ppermute(x, 'tp', [(i, step(i)) for i in range(n)])]
    unnamed x35 -> x47, local copies, waits for them, and re-layouts: 3.32 us -> 12.7 us
  transfers between devices with their start and end apart: 16 -> 20, of which waited for: 6 -> 5; matrix products, arithmetic and copies ran while one was open for 0% -> 0% of each run, Pallas kernels for 0% -> 0%
where the time goes in v1:
time: 201 us
  waiting for transfers between devices  94.9 us (47%)
  starting transfers between devices  35.7 us (18%)
  Pallas kernels  29.6 us (15%)
  blocking collectives  27.3 us (14%)
  local copies, waits for them, and re-layouts  12.8 us (6%)
    all_to_all x1, waiting for transfers between devices, local(): lax.all_to_all(result.reshape(x.shape), 'ep', split_axis=0, concat_axis=0...  51.3 us
    ppermute x18, waiting for transfers between devices, moved(): return lax.ppermute(x, 'tp', [(i, step(i)) for i in range(n)])  43.6 us
    ppermute x18, starting transfers between devices, moved(): return lax.ppermute(x, 'tp', [(i, step(i)) for i in range(n)])  20.5 us
    pallas_call x1, Pallas kernels, expert_unit(): pl.pallas_call(functools.partial(expert_kernel, gu_parts=tuple(((i, at, x...  19.5 us
    all_to_all x1, blocking collectives, local(): final = lax.all_to_all(mixed, 'tp', split_axis=0, concat_axis=0, tiled=True)  15.6 us
    unnamed x47, local copies, waits for them, and re-layouts  12.7 us
    all_gather x1, blocking collectives, local(): gain_full = lax.all_gather(out_gain, 'tp', axis=0, tiled=True)  11.7 us
    all_to_all x1, starting transfers between devices, local(): arrived = lax.all_to_all(x, 'ep', split_axis=0, concat_axis=0, tiled=True)  8.61 us
  transfers between devices with their start and end apart: 20, of which 5 were waited for; matrix products, arithmetic and copies ran while one was open for 0% of the time, Pallas kernels for 0%

profile of v1, /device:TPU:1, one launch (start us, length us, event | category | flops | bytes accessed | tf_op | source)
XLA Modules:
  0.0 200.8 jit_solution(16497156362650284781)
XLA Ops:
  0.0 4.6 %dispatch.1 = bf16[16,64,2048]{2,1,0:T(8,128)(2,1)} custom-call(s32[1]{0:T(128)} %bitcast.rank, bf16[128,2048]{1,0:T(8,128)(2,1)} %tokens_ref.1, s32[4,1024]{1,0:T(4,128)} %bitcast.21, f32[1,2048]{1,0:T(1,128)} %bitcast.25), custom_call_target="tpu_custom_call" | custom-call | tf_op jit(solution)/shard_map/dispatch/pallas_call | solution.py:62
  4.6 8.6 %all-to-all-start = ((bf16[16,64,2048]{2,1,0:T(8,128)(2,1)}), bf16[16,64,2048]{2,1,0:T(8,128)(2,1)}, u32[]{:S(2)}, u32[]{:S(2)}) async-start(bf16[16,64,2048]{2,1,0:T(8,128)(2,1)} %dispatch.1), calls=%async_computation | async-start | bytes 8388608 | tf_op jit(solution)/shard_map/all_to_all | solution.py:298
  13.3 0.1 pad_maximum_fusion.rest_0_
  13.4 1.4 collective-permute-start.1
  14.8 1.5 collective-permute-start.3
  16.3 0.0 collective-permute-start.10
  16.3 1.7 collective-permute-start
  18.0 2.6 %collective-permute-start.12 = (bf16[128,2048]{1,0:T(8,128)(2,1)S(1)}, bf16[128,2048]{1,0:T(8,128)(2,1)S(1)}, u32[]{:S(2)}, u32[]{:S(2)}) collective-permute-start(bf16[128,2048]{1,0:T(8,128)(2,1)S(1)} %bitcast.14), channel_id=1, source_target_pairs={{0,6},{1,7},{2,0},{3,1},{4,2},{5,3},{6,4},{7,5},{8,14},{9,15},{10,... | collective-permute-start | bytes 1572872 | tf_op jit(solution)/shard_map/ppermute | solution.py:263
  20.6 29.3 %collective-permute-done.10.rest_12_ = bf16[128,2048]{1,0:T(8,128)(2,1)S(1)} collective-permute-done((bf16[128,2048]{1,0:T(8,128)(2,1)S(1)}, bf16[128,2048]{1,0:T(8,128)(2,1)S(1)}, u32[]{:S(2)}, u32[]{:S(2)}) %collective-permute-start.10) | collective-permute-done | bytes 524320 | tf_op jit(solution)/shard_map/ppermute | solution.py:263
  49.9 1.6 collective-permute-start.9
  51.5 0.0 collective-permute-done.12.rest_14_
  51.5 0.0 collective-permute-start.11
  51.6 0.0 collective-permute-done.1.rest_2_
  51.6 1.4 collective-permute-start.14
  53.0 0.0 collective-permute-done.3.rest_4_
  53.0 1.5 collective-permute-start.15
  54.6 0.0 collective-permute-done.9.rest_11_
  54.6 1.0 collective-permute-start.13
  55.6 4.9 %collective-permute-done.14.rest_16_ = bf16[64,2048]{1,0:T(8,128)(2,1)S(1)} collective-permute-done((bf16[64,2048]{1,0:T(8,128)(2,1)S(1)}, bf16[64,2048]{1,0:T(8,128)(2,1)S(1)}, u32[]{:S(2)}, u32[]{:S(2)}) %collective-permute-start.14) | collective-permute-done | bytes 262176 | tf_op jit(solution)/shard_map/ppermute | solution.py:263
  60.5 0.5 collective-permute-start.5
  61.0 0.0 collective-permute-done.15.rest_17_
  61.0 1.0 collective-permute-start.2
  62.0 0.0 collective-permute-done.rest_1_
  62.0 0.1 collective-permute-start.4
  62.1 0.0 collective-permute-done.11.rest_13_
  62.1 2.7 %collective-permute-start.6 = (bf16[1024,256]{1,0:T(8,128)(2,1)S(1)}, bf16[1024,256]{1,0:T(8,128)(2,1)S(1)}, u32[]{:S(2)}, u32[]{:S(2)}) collective-permute-start(bf16[1024,256]{1,0:T(8,128)(2,1)S(1)} %slice.17), channel_id=1, source_target_pairs={{0,6},{1,7},{2,0},{3,1},{4,2},{5,3},{6,4},{7,5},{8,14},{9,15},{10,... | collective-permute-start | bytes 1572872 | tf_op jit(solution)/shard_map/ppermute | solution.py:263
  64.8 0.0 collective-permute-done.13.rest_15_
  64.8 0.7 collective-permute-start.16
  65.5 0.1 copy-done.22
  65.6 8.5 %collective-permute-done.5.rest_6_ = bf16[1024,256]{1,0:T(8,128)(2,1)S(1)} collective-permute-done((bf16[1024,256]{1,0:T(8,128)(2,1)S(1)}, bf16[1024,256]{1,0:T(8,128)(2,1)S(1)}, u32[]{:S(2)}, u32[]{:S(2)}) %collective-permute-start.5) | collective-permute-done | bytes 524320 | tf_op jit(solution)/shard_map/ppermute | solution.py:263
  74.1 1.9 collective-permute-start.7
  76.1 0.0 collective-permute-done.6.rest_7_
  76.1 0.8 collective-permute-start.8
  76.9 0.8 copy-done.1
  77.7 0.0 collective-permute-done.16.rest_18_
  77.7 0.7 copy-done.9
  78.4 0.0 collective-permute-start.17
  78.4 0.7 copy-done.7
  79.1 0.8 collective-permute-done.17.rest_19_
  79.9 0.7 copy-done.11
  80.7 0.0 collective-permute-done.2.rest_3_
  80.7 0.0 collective-permute-done.4.rest_5_
  80.7 0.0 collective-permute-done.7.rest_8_
  80.7 0.9 copy-done.20
  81.6 0.3 copy-done.21
  82.0 0.8 copy-done.3
  82.8 0.0 collective-permute-done.8.rest_9_
  82.8 0.8 copy-done.5
  83.6 0.0 all-to-all-done
  83.6 1.0 copy-done.2
  84.7 1.0 copy-done.4
  85.7 1.0 copy-done.6
  86.7 0.9 copy-done.8
  87.7 0.9 copy-done.10
  88.6 0.9 copy-done.12
  89.6 19.5 %expert_unit.1 = bf16[1024,2048]{1,0:T(8,128)(2,1)} custom-call(bf16[1024,2048]{1,0:T(8,128)(2,1)} %bitcast.6.rows_hbm, bf16[2048,256]{1,0:T(8,128)(2,1)} %copy-done.13, bf16[2048,256]{1,0:T(8,128)(2,1)} %copy-done.19, bf16[2048,256]{1,0:T(8,128)(2,1)} %copy-done.16, bf16[2048,256]{1,0:T(8,128)(2,1)} %copy-done.20, bf16[2048,256]{1,0:T(8,128)(2,1)} %copy-done.17, ...), custom_call_target="tpu_custom_call" | custom-call | flops 12884901888 | bytes 20971520 | tf_op jit(solution)/shard_map/expert_unit/pallas_call | solution.py:144
  109.1 0.0 copy-start.18
  109.2 6.7 %all-to-all-start.1 = ((bf16[16,64,2048]{2,1,0:T(8,128)(2,1)}), bf16[16,64,2048]{2,1,0:T(8,128)(2,1)}, u32[]{:S(2)}, u32[]{:S(2)}) async-start(bf16[16,64,2048]{2,1,0:T(8,128)(2,1)} %bitcast.17), calls=%async_computation.1 | async-start | bytes 8388608 | tf_op jit(solution)/shard_map/all_to_all | solution.py:300
  115.8 0.0 copy-done.18
  115.8 11.7 %all-gather = f32[8,1,256]{2,1,0:T(1,128)} all-gather(f32[1,1,256]{2,1,0:T(1,128)S(1)} %bitcast.26), channel_id=1, replica_groups=mesh['ep'=16,'tp'=8] {'tp'}, dimensions={0}, use_global_device_ids=true | all-gather | bytes 9216 | tf_op jit(solution)/shard_map/all_gather | solution.py:293
  127.6 51.3 %all-to-all-done.1 = bf16[16,64,2048]{2,1,0:T(8,128)(2,1)} async-done(((bf16[16,64,2048]{2,1,0:T(8,128)(2,1)}), bf16[16,64,2048]{2,1,0:T(8,128)(2,1)}, u32[]{:S(2)}, u32[]{:S(2)}) %all-to-all-start.1) | async-done | bytes 4194336 | tf_op jit(solution)/shard_map/all_to_all | solution.py:300
  178.9 5.5 %combine.1 = bf16[8,128,256]{2,1,0:T(8,128)(2,1)} custom-call(s32[1]{0:T(128)} %bitcast.rank, s32[4,1024]{1,0:T(4,128)} %bitcast.22, f32[4,1024]{1,0:T(4,128)} %bitcast.24, f32[1,2048]{1,0:T(1,128)} %bitcast.23, bf16[1024,2048]{1,0:T(8,128)(2,1)} %bitcast.11.rest_0_), custom_call_target="tpu_custom_call" | custom-call | tf_op jit(solution)/shard_map/combine/pallas_call | solution.py:237
  184.4 15.6 %all_to_all.15 = bf16[8,128,256]{2,1,0:T(8,128)(2,1)S(1)} all-to-all(bf16[8,128,256]{2,1,0:T(8,128)(2,1)} %combine.1), channel_id=1, replica_groups=mesh['ep'=16,'tp'=8] {'tp'}, dimensions={0} | all-to-all | bytes 1048576 | tf_op jit(solution)/shard_map/all_to_all | solution.py:307
  200.0 0.8 copy.10
  (33 shorter events, 0.2 us)
Async XLA Ops:
  4.6 8.6 %copy-start.14 = (bf16[1,2048,128]{2,1,0:T(8,128)(2,1)S(1)}, bf16[1,2048,128]{2,1,0:T(8,128)(2,1)}, u32[]{:S(2)}) copy-start(bf16[1,2048,128]{2,1,0:T(8,128)(2,1)} %param.13) | copy-start | bytes 1572868
  4.6 8.6 %copy-start.15 = (bf16[1,2048,128]{2,1,0:T(8,128)(2,1)S(1)}, bf16[1,2048,128]{2,1,0:T(8,128)(2,1)}, u32[]{:S(2)}) copy-start(bf16[1,2048,128]{2,1,0:T(8,128)(2,1)} %param.12) | copy-start | bytes 1572868
  4.6 11.7 %copy-start = (bf16[1,128,2048]{2,1,0:T(8,128)(2,1)S(1)}, bf16[1,128,2048]{2,1,0:T(8,128)(2,1)}, u32[]{:S(2)}) copy-start(bf16[1,128,2048]{2,1,0:T(8,128)(2,1)} %param.14) | copy-start | bytes 1572868
  4.6 79.0 %all-to-all-start = ((bf16[16,64,2048]{2,1,0:T(8,128)(2,1)}), bf16[16,64,2048]{2,1,0:T(8,128)(2,1)}, u32[]{:S(2)}, u32[]{:S(2)}) async-start(bf16[16,64,2048]{2,1,0:T(8,128)(2,1)} %dispatch.1), calls=%async_computation | async-start | bytes 8388608 | tf_op jit(solution)/shard_map/all_to_all | solution.py:298
  13.4 67.3 %copy-start.13 = (bf16[2048,256]{1,0:T(8,128)(2,1)}, bf16[2048,256]{1,0:T(8,128)(2,1)S(1)}, u32[]{:S(2)}) copy-start(bf16[2048,256]{1,0:T(8,128)(2,1)S(1)} %pad_maximum_fusion.rest_0_) | copy-start | bytes 3145732
  13.4 38.2 %collective-permute-start.1 = (bf16[2048,256]{1,0:T(8,128)(2,1)S(1)}, bf16[2048,256]{1,0:T(8,128)(2,1)S(1)}, u32[]{:S(2)}, u32[]{:S(2)}) collective-permute-start(bf16[2048,256]{1,0:T(8,128)(2,1)S(1)} %pad_maximum_fusion.rest_0_), channel_id=1, source_target_pairs={{0,2},{1,3},{2,4},{3,5},{4,6},{5,7},{6,0},{7,1},{8,10},{9,11},{10,... | collective-permute-start | bytes 3145736 | tf_op jit(solution)/shard_map/ppermute | solution.py:263
  14.8 38.2 %collective-permute-start.3 = (bf16[2048,256]{1,0:T(8,128)(2,1)S(1)}, bf16[2048,256]{1,0:T(8,128)(2,1)S(1)}, u32[]{:S(2)}, u32[]{:S(2)}) collective-permute-start(bf16[2048,256]{1,0:T(8,128)(2,1)S(1)} %pad_maximum_fusion.rest_0_), channel_id=1, source_target_pairs={{0,6},{1,7},{2,0},{3,1},{4,2},{5,3},{6,4},{7,5},{8,14},{9,15},{10,... | collective-permute-start | bytes 3145736 | tf_op jit(solution)/shard_map/ppermute | solution.py:263
  16.3 33.6 %collective-permute-start.10 = (bf16[128,2048]{1,0:T(8,128)(2,1)S(1)}, bf16[128,2048]{1,0:T(8,128)(2,1)S(1)}, u32[]{:S(2)}, u32[]{:S(2)}) collective-permute-start(bf16[128,2048]{1,0:T(8,128)(2,1)S(1)} %bitcast.13), channel_id=1, source_target_pairs={{0,2},{1,3},{2,4},{3,5},{4,6},{5,7},{6,0},{7,1},{8,10},{9,11},{10,... | collective-permute-start | bytes 1572872 | tf_op jit(solution)/shard_map/ppermute | solution.py:263
  16.3 45.7 %collective-permute-start = (bf16[2048,256]{1,0:T(8,128)(2,1)S(1)}, bf16[2048,256]{1,0:T(8,128)(2,1)S(1)}, u32[]{:S(2)}, u32[]{:S(2)}) collective-permute-start(bf16[2048,256]{1,0:T(8,128)(2,1)S(1)} %pad_maximum_fusion.rest_0_), channel_id=1, source_target_pairs={{0,1},{1,0},{2,3},{3,2},{4,5},{5,4},{6,7},{7,6},{8,9},{9,8},{10,11... | collective-permute-start | bytes 3145736 | tf_op jit(solution)/shard_map/ppermute | solution.py:263
  18.0 33.5 %collective-permute-start.12 = (bf16[128,2048]{1,0:T(8,128)(2,1)S(1)}, bf16[128,2048]{1,0:T(8,128)(2,1)S(1)}, u32[]{:S(2)}, u32[]{:S(2)}) collective-permute-start(bf16[128,2048]{1,0:T(8,128)(2,1)S(1)} %bitcast.14), channel_id=1, source_target_pairs={{0,6},{1,7},{2,0},{3,1},{4,2},{5,3},{6,4},{7,5},{8,14},{9,15},{10,... | collective-permute-start | bytes 1572872 | tf_op jit(solution)/shard_map/ppermute | solution.py:263
  49.9 4.7 %collective-permute-start.9 = (bf16[128,2048]{1,0:T(8,128)(2,1)S(1)}, bf16[128,2048]{1,0:T(8,128)(2,1)S(1)}, u32[]{:S(2)}, u32[]{:S(2)}) collective-permute-start(bf16[128,2048]{1,0:T(8,128)(2,1)S(1)} %bitcast.15), channel_id=1, source_target_pairs={{0,1},{1,0},{2,3},{3,2},{4,5},{5,4},{6,7},{7,6},{8,9},{9,8},{10,11... | collective-permute-start | bytes 1572872 | tf_op jit(solution)/shard_map/ppermute | solution.py:263
  51.5 10.6 %collective-permute-start.11 = (bf16[128,2048]{1,0:T(8,128)(2,1)S(1)}, bf16[128,2048]{1,0:T(8,128)(2,1)S(1)}, u32[]{:S(2)}, u32[]{:S(2)}) collective-permute-start(bf16[128,2048]{1,0:T(8,128)(2,1)S(1)} %collective-permute-done.10.rest_12_), channel_id=1, source_target_pairs={{0,1},{1,0},{2,3},{3,2},{4,5},{5,4},{6,7},{7,6},{8,9},{9,8},{10,11... | collective-permute-start | bytes 1572872 | tf_op jit(solution)/shard_map/ppermute | solution.py:263
  51.6 29.1 %copy-start.16 = (bf16[2048,256]{1,0:T(8,128)(2,1)}, bf16[2048,256]{1,0:T(8,128)(2,1)S(1)}, u32[]{:S(2)}) copy-start(bf16[2048,256]{1,0:T(8,128)(2,1)S(1)} %collective-permute-done.1.rest_2_) | copy-start | bytes 3145732
  51.6 8.9 %collective-permute-start.14 = (bf16[64,2048]{1,0:T(8,128)(2,1)S(1)}, bf16[64,2048]{1,0:T(8,128)(2,1)S(1)}, u32[]{:S(2)}, u32[]{:S(2)}) collective-permute-start(bf16[64,2048]{1,0:T(8,128)(2,1)S(1)} %slice.18), channel_id=1, source_target_pairs={{0,2},{1,3},{2,4},{3,5},{4,6},{5,7},{6,0},{7,1},{8,10},{9,11},{10,... | collective-permute-start | bytes 786440 | tf_op jit(solution)/shard_map/ppermute | solution.py:263
  53.0 27.7 %copy-start.17 = (bf16[2048,256]{1,0:T(8,128)(2,1)}, bf16[2048,256]{1,0:T(8,128)(2,1)S(1)}, u32[]{:S(2)}) copy-start(bf16[2048,256]{1,0:T(8,128)(2,1)S(1)} %collective-permute-done.3.rest_4_) | copy-start | bytes 3145732
  53.0 8.0 %collective-permute-start.15 = (bf16[64,2048]{1,0:T(8,128)(2,1)S(1)}, bf16[64,2048]{1,0:T(8,128)(2,1)S(1)}, u32[]{:S(2)}, u32[]{:S(2)}) collective-permute-start(bf16[64,2048]{1,0:T(8,128)(2,1)S(1)} %slice.19), channel_id=1, source_target_pairs={{0,6},{1,7},{2,0},{3,1},{4,2},{5,3},{6,4},{7,5},{8,14},{9,15},{10,... | collective-permute-start | bytes 786440 | tf_op jit(solution)/shard_map/ppermute | solution.py:263
  54.6 10.1 %collective-permute-start.13 = (bf16[128,2048]{1,0:T(8,128)(2,1)S(1)}, bf16[128,2048]{1,0:T(8,128)(2,1)S(1)}, u32[]{:S(2)}, u32[]{:S(2)}) collective-permute-start(bf16[128,2048]{1,0:T(8,128)(2,1)S(1)} %collective-permute-done.12.rest_14_), channel_id=1, source_target_pairs={{0,1},{1,0},{2,3},{3,2},{4,5},{5,4},{6,7},{7,6},{8,9},{9,8},{10,11... | collective-permute-start | bytes 1572872 | tf_op jit(solution)/shard_map/ppermute | solution.py:263
  60.5 13.6 %collective-permute-start.5 = (bf16[1024,256]{1,0:T(8,128)(2,1)S(1)}, bf16[1024,256]{1,0:T(8,128)(2,1)S(1)}, u32[]{:S(2)}, u32[]{:S(2)}) collective-permute-start(bf16[1024,256]{1,0:T(8,128)(2,1)S(1)} %slice.16), channel_id=1, source_target_pairs={{0,2},{1,3},{2,4},{3,5},{4,6},{5,7},{6,0},{7,1},{8,10},{9,11},{10,... | collective-permute-start | bytes 1572872 | tf_op jit(solution)/shard_map/ppermute | solution.py:263
  61.0 19.7 %collective-permute-start.2 = (bf16[2048,256]{1,0:T(8,128)(2,1)S(1)}, bf16[2048,256]{1,0:T(8,128)(2,1)S(1)}, u32[]{:S(2)}, u32[]{:S(2)}) collective-permute-start(bf16[2048,256]{1,0:T(8,128)(2,1)S(1)} %collective-permute-done.1.rest_2_), channel_id=1, source_target_pairs={{0,1},{1,0},{2,3},{3,2},{4,5},{5,4},{6,7},{7,6},{8,9},{9,8},{10,11... | collective-permute-start | bytes 3145736 | tf_op jit(solution)/shard_map/ppermute | solution.py:263
  62.0 18.7 %copy-start.19 = (bf16[2048,256]{1,0:T(8,128)(2,1)}, bf16[2048,256]{1,0:T(8,128)(2,1)S(1)}, u32[]{:S(2)}) copy-start(bf16[2048,256]{1,0:T(8,128)(2,1)S(1)} %collective-permute-done.rest_1_) | copy-start | bytes 3145732
  62.0 18.6 %collective-permute-start.4 = (bf16[2048,256]{1,0:T(8,128)(2,1)S(1)}, bf16[2048,256]{1,0:T(8,128)(2,1)S(1)}, u32[]{:S(2)}, u32[]{:S(2)}) collective-permute-start(bf16[2048,256]{1,0:T(8,128)(2,1)S(1)} %collective-permute-done.3.rest_4_), channel_id=1, source_target_pairs={{0,1},{1,0},{2,3},{3,2},{4,5},{5,4},{6,7},{7,6},{8,9},{9,8},{10,11... | collective-permute-start | bytes 3145736 | tf_op jit(solution)/shard_map/ppermute | solution.py:263
  62.1 14.0 %collective-permute-start.6 = (bf16[1024,256]{1,0:T(8,128)(2,1)S(1)}, bf16[1024,256]{1,0:T(8,128)(2,1)S(1)}, u32[]{:S(2)}, u32[]{:S(2)}) collective-permute-start(bf16[1024,256]{1,0:T(8,128)(2,1)S(1)} %slice.17), channel_id=1, source_target_pairs={{0,6},{1,7},{2,0},{3,1},{4,2},{5,3},{6,4},{7,5},{8,14},{9,15},{10,... | collective-permute-start | bytes 1572872 | tf_op jit(solution)/shard_map/ppermute | solution.py:263
  64.8 0.8 copy-start.22
  64.8 12.9 %collective-permute-start.16 = (bf16[64,2048]{1,0:T(8,128)(2,1)S(1)}, bf16[64,2048]{1,0:T(8,128)(2,1)S(1)}, u32[]{:S(2)}, u32[]{:S(2)}) collective-permute-start(bf16[64,2048]{1,0:T(8,128)(2,1)S(1)} %collective-permute-done.14.rest_16_), channel_id=1, source_target_pairs={{0,1},{1,0},{2,3},{3,2},{4,5},{5,4},{6,7},{7,6},{8,9},{9,8},{10,11... | collective-permute-start | bytes 786440 | tf_op jit(solution)/shard_map/ppermute | solution.py:263
  74.1 6.5 %collective-permute-start.7 = (bf16[1024,256]{1,0:T(8,128)(2,1)S(1)}, bf16[1024,256]{1,0:T(8,128)(2,1)S(1)}, u32[]{:S(2)}, u32[]{:S(2)}) collective-permute-start(bf16[1024,256]{1,0:T(8,128)(2,1)S(1)} %collective-permute-done.5.rest_6_), channel_id=1, source_target_pairs={{0,1},{1,0},{2,3},{3,2},{4,5},{5,4},{6,7},{7,6},{8,9},{9,8},{10,11... | collective-permute-start | bytes 1572872 | tf_op jit(solution)/shard_map/ppermute | solution.py:263
  76.1 6.7 %collective-permute-start.8 = (bf16[1024,256]{1,0:T(8,128)(2,1)S(1)}, bf16[1024,256]{1,0:T(8,128)(2,1)S(1)}, u32[]{:S(2)}, u32[]{:S(2)}) collective-permute-start(bf16[1024,256]{1,0:T(8,128)(2,1)S(1)} %collective-permute-done.6.rest_7_), channel_id=1, source_target_pairs={{0,1},{1,0},{2,3},{3,2},{4,5},{5,4},{6,7},{7,6},{8,9},{9,8},{10,11... | collective-permute-start | bytes 1572872 | tf_op jit(solution)/shard_map/ppermute | solution.py:263
  76.9 0.8 copy-start.1
  77.7 0.7 copy-start.9
  78.4 1.5 collective-permute-start.17
  78.4 0.7 copy-start.7
  79.9 0.7 copy-start.11
  80.7 1.0 copy-start.20
  80.7 1.3 copy-start.21
  82.0 0.8 copy-start.3
  82.8 0.8 copy-start.5
  83.6 1.0 copy-start.2
  84.7 1.0 copy-start.4
  85.7 1.0 copy-start.6
  86.7 0.9 copy-start.8
  87.7 0.9 copy-start.10
  88.6 0.9 copy-start.12
  109.1 6.7 %copy-start.18 = (f32[256]{0:T(256)S(1)}, f32[256]{0:T(256)}, u32[]{:S(2)}) copy-start(f32[256]{0:T(256)} %param.15) | copy-start | bytes 3076
  109.2 69.7 %all-to-all-start.1 = ((bf16[16,64,2048]{2,1,0:T(8,128)(2,1)}), bf16[16,64,2048]{2,1,0:T(8,128)(2,1)}, u32[]{:S(2)}, u32[]{:S(2)}) async-start(bf16[16,64,2048]{2,1,0:T(8,128)(2,1)} %bitcast.17), calls=%async_computation.1 | async-start | bytes 8388608 | tf_op jit(solution)/shard_map/all_to_all | solution.py:300

commit v2 on v1

--- a/solution.py
+++ b/solution.py
@@ -161,7 +161,7 @@
             pltpu.SemaphoreType.DMA((len(dn),)),
             pltpu.SemaphoreType.DMA((4,)),
         ],
-        compiler_params=pltpu.CompilerParams(vmem_limit_bytes=48 * 2**20),
+        compiler_params=pltpu.CompilerParams(vmem_limit_bytes=60 * 2**20),
         cost_estimate=pl.CostEstimate(
             flops=6 * total * width * parts * hid, bytes_accessed=20 * 2**20, transcendentals=total * parts * hid
         ),
@@ -209,7 +209,7 @@
             for q in range(per):
                 hit = (owner == q) & (col == table[:, e + q : e + q + 1])
                 spread = jnp.where(hit, table[:, experts + e + q : experts + e + q + 1], spread)
-            for p in range(3):
+            for p in range(2):
                 part = spread.astype(bf16)
                 spread_v[p * tokens : (p + 1) * tokens, base : base + lanes] = part
                 spread = spread - part.astype(f32)
@@ -221,7 +221,7 @@
             copy.wait()
         span = pl.ds(c * cols, cols)
         prod = jnp.dot(spread_v[...], back_v[:, span], preferred_element_type=f32)
-        combined = prod[:tokens] + prod[tokens : 2 * tokens] + prod[2 * tokens :]
+        combined = prod[:tokens] + prod[tokens:]
         total_sq = total_sq + jnp.sum(combined * combined, axis=-1, keepdims=True)
         acc_v[:, span] = combined
     scale = lax.rsqrt(total_sq / width + epsilon)
@@ -249,7 +249,7 @@
             out_specs=pl.BlockSpec((slices, rows, width // slices), lambda s, r: (0, 0, 0)),
             scratch_shapes=[
                 pltpu.VMEM((experts * sum(split), width), bf16),
-                pltpu.VMEM((3 * rows, experts * sum(split)), bf16),
+                pltpu.VMEM((2 * rows, experts * sum(split)), bf16),
                 pltpu.VMEM((rows, width), f32),
                 pltpu.SemaphoreType.DMA((len(split), 4)),
             ],

time: 201 us -> 192 us (0.955)
  local copies, waits for them, and re-layouts: 12.8 us -> 3.08 us
    unnamed x47 -> x43, local copies, waits for them, and re-layouts: 12.7 us -> 2.97 us
where the time goes in v2:
time: 192 us; the launch traced here: 191 us
  waiting for transfers between devices  95.2 us (50%)
  starting transfers between devices  36 us (19%)
  Pallas kernels  28.6 us (15%)
  blocking collectives  27.9 us (15%)
  local copies, waits for them, and re-layouts  3.08 us (2%)
    all_to_all x1, waiting for transfers between devices, local(): lax.all_to_all(result.reshape(x.shape), 'ep', split_axis=0, concat_axis=0...  50.6 us
    ppermute x18, waiting for transfers between devices, moved(): return lax.ppermute(x, 'tp', [(i, step(i)) for i in range(n)])  44.6 us
    ppermute x18, starting transfers between devices, moved(): return lax.ppermute(x, 'tp', [(i, step(i)) for i in range(n)])  20.7 us
    pallas_call x1, Pallas kernels, expert_unit(): pl.pallas_call(functools.partial(expert_kernel, gu_parts=tuple(((i, at, x...  19.1 us
    all_to_all x1, blocking collectives, local(): final = lax.all_to_all(mixed, 'tp', split_axis=0, concat_axis=0, tiled=True)  15.8 us
    all_gather x1, blocking collectives, local(): gain_full = lax.all_gather(out_gain, 'tp', axis=0, tiled=True)  12.1 us
    all_to_all x1, starting transfers between devices, local(): arrived = lax.all_to_all(x, 'ep', split_axis=0, concat_axis=0, tiled=True)  8.6 us
    all_to_all x1, starting transfers between devices, local(): lax.all_to_all(result.reshape(x.shape), 'ep', split_axis=0, concat_axis=0...  6.67 us
  transfers between devices with their start and end apart: 20, of which 5 were waited for; matrix products, arithmetic and copies ran while one was open for 0% of the time, Pallas kernels for 0%

profile of v2, /device:TPU:1, one launch (start us, length us, event | category | flops | bytes accessed | tf_op | source)
XLA Modules:
  0.0 191.2 jit_solution(5397993468132568936)
XLA Ops:
  0.0 4.6 %dispatch.1 = bf16[16,64,2048]{2,1,0:T(8,128)(2,1)} custom-call(s32[1]{0:T(128)} %bitcast.rank, bf16[128,2048]{1,0:T(8,128)(2,1)} %tokens_ref.1, s32[4,1024]{1,0:T(4,128)} %bitcast.17, f32[1,2048]{1,0:T(1,128)} %bitcast.21), custom_call_target="tpu_custom_call" | custom-call | tf_op jit(solution)/shard_map/dispatch/pallas_call | solution.py:62
  4.6 8.6 %all-to-all-start = ((bf16[16,64,2048]{2,1,0:T(8,128)(2,1)}), bf16[16,64,2048]{2,1,0:T(8,128)(2,1)}, u32[]{:S(2)}, u32[]{:S(2)}) async-start(bf16[16,64,2048]{2,1,0:T(8,128)(2,1)} %dispatch.1), calls=%async_computation | async-start | bytes 8388608 | tf_op jit(solution)/shard_map/all_to_all | solution.py:298
  13.2 0.0 copy-done.1
  13.2 0.0 copy-done.2
  13.2 0.1 pad_maximum_fusion.rest_0_
  13.3 0.0 copy-start
  13.3 1.4 collective-permute-start.1
  14.7 1.5 collective-permute-start.3
  16.2 0.0 collective-permute-start.10
  16.2 1.7 collective-permute-start
  17.9 2.6 %collective-permute-start.12 = (bf16[128,2048]{1,0:T(8,128)(2,1)}, bf16[128,2048]{1,0:T(8,128)(2,1)S(1)}, u32[]{:S(2)}, u32[]{:S(2)}) collective-permute-start(bf16[128,2048]{1,0:T(8,128)(2,1)} %bitcast.24), channel_id=1, source_target_pairs={{0,6},{1,7},{2,0},{3,1},{4,2},{5,3},{6,4},{7,5},{8,14},{9,15},{10,... | collective-permute-start | bytes 1572872 | tf_op jit(solution)/shard_map/ppermute | solution.py:263
  20.5 29.3 %collective-permute-done.10.rest_12_ = bf16[128,2048]{1,0:T(8,128)(2,1)S(1)} collective-permute-done((bf16[128,2048]{1,0:T(8,128)(2,1)}, bf16[128,2048]{1,0:T(8,128)(2,1)S(1)}, u32[]{:S(2)}, u32[]{:S(2)}) %collective-permute-start.10) | collective-permute-done | bytes 524320 | tf_op jit(solution)/shard_map/ppermute | solution.py:263
  49.8 1.6 collective-permute-start.9
  51.5 0.0 collective-permute-done.12.rest_14_
  51.5 0.1 collective-permute-start.11
  51.6 0.0 collective-permute-done.1.rest_2_
  51.6 0.0 copy-start.3
  51.6 1.3 collective-permute-start.14
  52.9 0.0 collective-permute-done.3.rest_4_
  52.9 1.5 collective-permute-start.15
  54.6 0.0 collective-permute-done.9.rest_11_
  54.6 0.0 copy-start.11
  54.6 1.0 collective-permute-start.13
  55.6 4.9 %collective-permute-done.14.rest_16_ = bf16[64,2048]{1,0:T(8,128)(2,1)S(1)} collective-permute-done((bf16[64,2048]{1,0:T(8,128)(2,1)S(1)}, bf16[64,2048]{1,0:T(8,128)(2,1)S(1)}, u32[]{:S(2)}, u32[]{:S(2)}) %collective-permute-start.14) | collective-permute-done | bytes 262176 | tf_op jit(solution)/shard_map/ppermute | solution.py:263
  60.5 0.4 collective-permute-start.5
  60.9 0.0 collective-permute-done.15.rest_17_
  60.9 1.0 collective-permute-start.2
  61.9 0.0 collective-permute-done.rest_1_
  62.0 0.1 collective-permute-start.4
  62.1 0.0 collective-permute-done.11.rest_13_
  62.1 2.7 %collective-permute-start.6 = (bf16[1024,256]{1,0:T(8,128)(2,1)S(1)}, bf16[1024,256]{1,0:T(8,128)(2,1)S(1)}, u32[]{:S(2)}, u32[]{:S(2)}) collective-permute-start(bf16[1024,256]{1,0:T(8,128)(2,1)S(1)} %slice.17), channel_id=1, source_target_pairs={{0,6},{1,7},{2,0},{3,1},{4,2},{5,3},{6,4},{7,5},{8,14},{9,15},{10,... | collective-permute-start | bytes 1572872 | tf_op jit(solution)/shard_map/ppermute | solution.py:263
  64.7 0.0 collective-permute-done.13.rest_15_
  64.7 0.7 collective-permute-start.16
  65.4 8.7 %collective-permute-done.5.rest_6_ = bf16[1024,256]{1,0:T(8,128)(2,1)S(1)} collective-permute-done((bf16[1024,256]{1,0:T(8,128)(2,1)S(1)}, bf16[1024,256]{1,0:T(8,128)(2,1)S(1)}, u32[]{:S(2)}, u32[]{:S(2)}) %collective-permute-start.5) | collective-permute-done | bytes 524320 | tf_op jit(solution)/shard_map/ppermute | solution.py:263
  74.1 1.9 %collective-permute-start.7 = (bf16[1024,256]{1,0:T(8,128)(2,1)S(1)}, bf16[1024,256]{1,0:T(8,128)(2,1)S(1)}, u32[]{:S(2)}, u32[]{:S(2)}) collective-permute-start(bf16[1024,256]{1,0:T(8,128)(2,1)S(1)} %collective-permute-done.5.rest_6_), channel_id=1, source_target_pairs={{0,1},{1,0},{2,3},{3,2},{4,5},{5,4},{6,7},{7,6},{8,9},{9,8},{10,11... | collective-permute-start | bytes 1572872 | tf_op jit(solution)/shard_map/ppermute | solution.py:263
  76.0 0.0 collective-permute-done.6.rest_7_
  76.0 0.8 collective-permute-start.8
  76.9 0.0 collective-permute-done.16.rest_18_
  76.9 0.3 collective-permute-start.17
  77.1 1.6 collective-permute-done.17.rest_19_
  78.8 0.0 collective-permute-done.2.rest_3_
  78.8 0.0 collective-permute-done.4.rest_5_
  78.8 0.0 copy-done.5
  78.8 0.0 copy-start.10
  78.8 0.0 collective-permute-done.7.rest_8_
  78.8 0.0 copy-done.6
  78.8 0.0 copy-done.11
  78.8 0.0 copy-done.18
  78.9 0.0 copy-done.8
  78.9 0.0 copy-done.12
  78.9 0.6 copy-done.20
  79.5 0.4 copy-done.9
  79.9 0.3 copy-done.10
  80.2 0.8 copy-done.16
  81.0 0.0 collective-permute-done.8.rest_9_
  81.0 0.0 all-to-all-done
  81.1 19.1 %expert_unit.1 = bf16[1024,2048]{1,0:T(8,128)(2,1)} custom-call(bf16[1024,2048]{1,0:T(8,128)(2,1)} %bitcast.6.rows_hbm, bf16[2048,256]{1,0:T(8,128)(2,1)} %copy-done, bf16[2048,256]{1,0:T(8,128)(2,1)} %copy-done.8, bf16[2048,256]{1,0:T(8,128)(2,1)} %copy-done.3, bf16[2048,256]{1,0:T(8,128)(2,1)} %copy-done.9, bf16[2048,256]{1,0:T(8,128)(2,1)} %copy-done.4, ...), custom_call_target="tpu_custom_call" | custom-call | flops 12884901888 | bytes 20971520 | tf_op jit(solution)/shard_map/expert_unit/pallas_call | solution.py:144
  100.2 0.0 copy-start.7
  100.2 6.7 %all-to-all-start.1 = ((bf16[16,64,2048]{2,1,0:T(8,128)(2,1)}), bf16[16,64,2048]{2,1,0:T(8,128)(2,1)}, u32[]{:S(2)}, u32[]{:S(2)}) async-start(bf16[16,64,2048]{2,1,0:T(8,128)(2,1)} %bitcast.13), calls=%async_computation.1 | async-start | bytes 8388608 | tf_op jit(solution)/shard_map/all_to_all | solution.py:300
  106.9 12.1 %all-gather = f32[8,1,256]{2,1,0:T(1,128)} all-gather(f32[1,1,256]{2,1,0:T(1,128)S(1)} %bitcast.22), channel_id=1, replica_groups=mesh['ep'=16,'tp'=8] {'tp'}, dimensions={0}, use_global_device_ids=true | all-gather | bytes 9216 | tf_op jit(solution)/shard_map/all_gather | solution.py:293
  119.0 50.6 %all-to-all-done.1 = bf16[16,64,2048]{2,1,0:T(8,128)(2,1)} async-done(((bf16[16,64,2048]{2,1,0:T(8,128)(2,1)}), bf16[16,64,2048]{2,1,0:T(8,128)(2,1)}, u32[]{:S(2)}, u32[]{:S(2)}) %all-to-all-start.1) | async-done | bytes 4194336 | tf_op jit(solution)/shard_map/all_to_all | solution.py:300
  169.7 4.9 %combine.1 = bf16[8,128,256]{2,1,0:T(8,128)(2,1)} custom-call(s32[1]{0:T(128)} %bitcast.rank, s32[4,1024]{1,0:T(4,128)} %bitcast.18, f32[4,1024]{1,0:T(4,128)} %bitcast.20, f32[1,2048]{1,0:T(1,128)} %bitcast.19, bf16[1024,2048]{1,0:T(8,128)(2,1)} %bitcast.11.rest_0_), custom_call_target="tpu_custom_call" | custom-call | tf_op jit(solution)/shard_map/combine/pallas_call | solution.py:237
  174.6 15.8 %all_to_all.15 = bf16[8,128,256]{2,1,0:T(8,128)(2,1)S(1)} all-to-all(bf16[8,128,256]{2,1,0:T(8,128)(2,1)} %combine.1), channel_id=1, replica_groups=mesh['ep'=16,'tp'=8] {'tp'}, dimensions={0} | all-to-all | bytes 1048576 | tf_op jit(solution)/shard_map/all_to_all | solution.py:307
  190.4 0.8 copy.10
  (29 shorter events, 0.2 us)
Async XLA Ops:
  4.6 8.6 %copy-start.1 = (bf16[1,2048,128]{2,1,0:T(8,128)(2,1)S(1)}, bf16[1,2048,128]{2,1,0:T(8,128)(2,1)}, u32[]{:S(2)}) copy-start(bf16[1,2048,128]{2,1,0:T(8,128)(2,1)} %param.13) | copy-start | bytes 1572868
  4.6 8.6 %copy-start.2 = (bf16[1,2048,128]{2,1,0:T(8,128)(2,1)S(1)}, bf16[1,2048,128]{2,1,0:T(8,128)(2,1)}, u32[]{:S(2)}) copy-start(bf16[1,2048,128]{2,1,0:T(8,128)(2,1)} %param.12) | copy-start | bytes 1572868
  4.6 76.5 %all-to-all-start = ((bf16[16,64,2048]{2,1,0:T(8,128)(2,1)}), bf16[16,64,2048]{2,1,0:T(8,128)(2,1)}, u32[]{:S(2)}, u32[]{:S(2)}) async-start(bf16[16,64,2048]{2,1,0:T(8,128)(2,1)} %dispatch.1), calls=%async_computation | async-start | bytes 8388608 | tf_op jit(solution)/shard_map/all_to_all | solution.py:298
  13.3 67.7 %copy-start = (bf16[2048,256]{1,0:T(8,128)(2,1)}, bf16[2048,256]{1,0:T(8,128)(2,1)S(1)}, u32[]{:S(2)}) copy-start(bf16[2048,256]{1,0:T(8,128)(2,1)S(1)} %pad_maximum_fusion.rest_0_) | copy-start | bytes 3145732
  13.3 38.3 %collective-permute-start.1 = (bf16[2048,256]{1,0:T(8,128)(2,1)S(1)}, bf16[2048,256]{1,0:T(8,128)(2,1)S(1)}, u32[]{:S(2)}, u32[]{:S(2)}) collective-permute-start(bf16[2048,256]{1,0:T(8,128)(2,1)S(1)} %pad_maximum_fusion.rest_0_), channel_id=1, source_target_pairs={{0,2},{1,3},{2,4},{3,5},{4,6},{5,7},{6,0},{7,1},{8,10},{9,11},{10,... | collective-permute-start | bytes 3145736 | tf_op jit(solution)/shard_map/ppermute | solution.py:263
  14.7 38.3 %collective-permute-start.3 = (bf16[2048,256]{1,0:T(8,128)(2,1)S(1)}, bf16[2048,256]{1,0:T(8,128)(2,1)S(1)}, u32[]{:S(2)}, u32[]{:S(2)}) collective-permute-start(bf16[2048,256]{1,0:T(8,128)(2,1)S(1)} %pad_maximum_fusion.rest_0_), channel_id=1, source_target_pairs={{0,6},{1,7},{2,0},{3,1},{4,2},{5,3},{6,4},{7,5},{8,14},{9,15},{10,... | collective-permute-start | bytes 3145736 | tf_op jit(solution)/shard_map/ppermute | solution.py:263
  16.2 33.6 %collective-permute-start.10 = (bf16[128,2048]{1,0:T(8,128)(2,1)}, bf16[128,2048]{1,0:T(8,128)(2,1)S(1)}, u32[]{:S(2)}, u32[]{:S(2)}) collective-permute-start(bf16[128,2048]{1,0:T(8,128)(2,1)} %bitcast.23), channel_id=1, source_target_pairs={{0,2},{1,3},{2,4},{3,5},{4,6},{5,7},{6,0},{7,1},{8,10},{9,11},{10,... | collective-permute-start | bytes 1572872 | tf_op jit(solution)/shard_map/ppermute | solution.py:263
  16.2 45.7 %collective-permute-start = (bf16[2048,256]{1,0:T(8,128)(2,1)S(1)}, bf16[2048,256]{1,0:T(8,128)(2,1)S(1)}, u32[]{:S(2)}, u32[]{:S(2)}) collective-permute-start(bf16[2048,256]{1,0:T(8,128)(2,1)S(1)} %pad_maximum_fusion.rest_0_), channel_id=1, source_target_pairs={{0,1},{1,0},{2,3},{3,2},{4,5},{5,4},{6,7},{7,6},{8,9},{9,8},{10,11... | collective-permute-start | bytes 3145736 | tf_op jit(solution)/shard_map/ppermute | solution.py:263
  17.9 33.5 %collective-permute-start.12 = (bf16[128,2048]{1,0:T(8,128)(2,1)}, bf16[128,2048]{1,0:T(8,128)(2,1)S(1)}, u32[]{:S(2)}, u32[]{:S(2)}) collective-permute-start(bf16[128,2048]{1,0:T(8,128)(2,1)} %bitcast.24), channel_id=1, source_target_pairs={{0,6},{1,7},{2,0},{3,1},{4,2},{5,3},{6,4},{7,5},{8,14},{9,15},{10,... | collective-permute-start | bytes 1572872 | tf_op jit(solution)/shard_map/ppermute | solution.py:263
  49.8 29.0 %copy-start.5 = (bf16[128,2048]{1,0:T(8,128)(2,1)}, bf16[128,2048]{1,0:T(8,128)(2,1)S(1)}, u32[]{:S(2)}) copy-start(bf16[128,2048]{1,0:T(8,128)(2,1)S(1)} %collective-permute-done.10.rest_12_) | copy-start | bytes 1572868
  49.8 4.7 %collective-permute-start.9 = (bf16[128,2048]{1,0:T(8,128)(2,1)}, bf16[128,2048]{1,0:T(8,128)(2,1)S(1)}, u32[]{:S(2)}, u32[]{:S(2)}) collective-permute-start(bf16[128,2048]{1,0:T(8,128)(2,1)} %bitcast.25), channel_id=1, source_target_pairs={{0,1},{1,0},{2,3},{3,2},{4,5},{5,4},{6,7},{7,6},{8,9},{9,8},{10,11... | collective-permute-start | bytes 1572872 | tf_op jit(solution)/shard_map/ppermute | solution.py:263
  51.5 27.3 %copy-start.6 = (bf16[128,2048]{1,0:T(8,128)(2,1)}, bf16[128,2048]{1,0:T(8,128)(2,1)S(1)}, u32[]{:S(2)}) copy-start(bf16[128,2048]{1,0:T(8,128)(2,1)S(1)} %collective-permute-done.12.rest_14_) | copy-start | bytes 1572868
  51.5 10.6 %collective-permute-start.11 = (bf16[128,2048]{1,0:T(8,128)(2,1)S(1)}, bf16[128,2048]{1,0:T(8,128)(2,1)S(1)}, u32[]{:S(2)}, u32[]{:S(2)}) collective-permute-start(bf16[128,2048]{1,0:T(8,128)(2,1)S(1)} %collective-permute-done.10.rest_12_), channel_id=1, source_target_pairs={{0,1},{1,0},{2,3},{3,2},{4,5},{5,4},{6,7},{7,6},{8,9},{9,8},{10,11... | collective-permute-start | bytes 1572872 | tf_op jit(solution)/shard_map/ppermute | solution.py:263
  51.6 29.4 %copy-start.3 = (bf16[2048,256]{1,0:T(8,128)(2,1)}, bf16[2048,256]{1,0:T(8,128)(2,1)S(1)}, u32[]{:S(2)}) copy-start(bf16[2048,256]{1,0:T(8,128)(2,1)S(1)} %collective-permute-done.1.rest_2_) | copy-start | bytes 3145732
  51.6 8.8 %collective-permute-start.14 = (bf16[64,2048]{1,0:T(8,128)(2,1)S(1)}, bf16[64,2048]{1,0:T(8,128)(2,1)S(1)}, u32[]{:S(2)}, u32[]{:S(2)}) collective-permute-start(bf16[64,2048]{1,0:T(8,128)(2,1)S(1)} %slice.18), channel_id=1, source_target_pairs={{0,2},{1,3},{2,4},{3,5},{4,6},{5,7},{6,0},{7,1},{8,10},{9,11},{10,... | collective-permute-start | bytes 786440 | tf_op jit(solution)/shard_map/ppermute | solution.py:263
  52.9 28.1 %copy-start.4 = (bf16[2048,256]{1,0:T(8,128)(2,1)}, bf16[2048,256]{1,0:T(8,128)(2,1)S(1)}, u32[]{:S(2)}) copy-start(bf16[2048,256]{1,0:T(8,128)(2,1)S(1)} %collective-permute-done.3.rest_4_) | copy-start | bytes 3145732
  52.9 8.0 %collective-permute-start.15 = (bf16[64,2048]{1,0:T(8,128)(2,1)S(1)}, bf16[64,2048]{1,0:T(8,128)(2,1)S(1)}, u32[]{:S(2)}, u32[]{:S(2)}) collective-permute-start(bf16[64,2048]{1,0:T(8,128)(2,1)S(1)} %slice.19), channel_id=1, source_target_pairs={{0,6},{1,7},{2,0},{3,1},{4,2},{5,3},{6,4},{7,5},{8,14},{9,15},{10,... | collective-permute-start | bytes 786440 | tf_op jit(solution)/shard_map/ppermute | solution.py:263
  54.6 24.3 %copy-start.11 = (bf16[128,2048]{1,0:T(8,128)(2,1)}, bf16[128,2048]{1,0:T(8,128)(2,1)S(1)}, u32[]{:S(2)}) copy-start(bf16[128,2048]{1,0:T(8,128)(2,1)S(1)} %collective-permute-done.9.rest_11_) | copy-start | bytes 1572868
  54.6 10.2 %collective-permute-start.13 = (bf16[128,2048]{1,0:T(8,128)(2,1)S(1)}, bf16[128,2048]{1,0:T(8,128)(2,1)S(1)}, u32[]{:S(2)}, u32[]{:S(2)}) collective-permute-start(bf16[128,2048]{1,0:T(8,128)(2,1)S(1)} %collective-permute-done.12.rest_14_), channel_id=1, source_target_pairs={{0,1},{1,0},{2,3},{3,2},{4,5},{5,4},{6,7},{7,6},{8,9},{9,8},{10,11... | collective-permute-start | bytes 1572872 | tf_op jit(solution)/shard_map/ppermute | solution.py:263
  60.5 20.6 %copy-start.17 = (bf16[64,2048]{1,0:T(8,128)(2,1)}, bf16[64,2048]{1,0:T(8,128)(2,1)S(1)}, u32[]{:S(2)}) copy-start(bf16[64,2048]{1,0:T(8,128)(2,1)S(1)} %collective-permute-done.14.rest_16_) | copy-start | bytes 786436
  60.5 13.6 %collective-permute-start.5 = (bf16[1024,256]{1,0:T(8,128)(2,1)S(1)}, bf16[1024,256]{1,0:T(8,128)(2,1)S(1)}, u32[]{:S(2)}, u32[]{:S(2)}) collective-permute-start(bf16[1024,256]{1,0:T(8,128)(2,1)S(1)} %slice.16), channel_id=1, source_target_pairs={{0,2},{1,3},{2,4},{3,5},{4,6},{5,7},{6,0},{7,1},{8,10},{9,11},{10,... | collective-permute-start | bytes 1572872 | tf_op jit(solution)/shard_map/ppermute | solution.py:263
  60.9 17.9 %copy-start.18 = (bf16[64,2048]{1,0:T(8,128)(2,1)}, bf16[64,2048]{1,0:T(8,128)(2,1)S(1)}, u32[]{:S(2)}) copy-start(bf16[64,2048]{1,0:T(8,128)(2,1)S(1)} %collective-permute-done.15.rest_17_) | copy-start | bytes 786436
  60.9 17.9 %collective-permute-start.2 = (bf16[2048,256]{1,0:T(8,128)(2,1)S(1)}, bf16[2048,256]{1,0:T(8,128)(2,1)S(1)}, u32[]{:S(2)}, u32[]{:S(2)}) collective-permute-start(bf16[2048,256]{1,0:T(8,128)(2,1)S(1)} %collective-permute-done.1.rest_2_), channel_id=1, source_target_pairs={{0,1},{1,0},{2,3},{3,2},{4,5},{5,4},{6,7},{7,6},{8,9},{9,8},{10,11... | collective-permute-start | bytes 3145736 | tf_op jit(solution)/shard_map/ppermute | solution.py:263
  62.0 16.9 %copy-start.8 = (bf16[2048,256]{1,0:T(8,128)(2,1)}, bf16[2048,256]{1,0:T(8,128)(2,1)S(1)}, u32[]{:S(2)}) copy-start(bf16[2048,256]{1,0:T(8,128)(2,1)S(1)} %collective-permute-done.rest_1_) | copy-start | bytes 3145732
  62.0 16.8 %collective-permute-start.4 = (bf16[2048,256]{1,0:T(8,128)(2,1)S(1)}, bf16[2048,256]{1,0:T(8,128)(2,1)S(1)}, u32[]{:S(2)}, u32[]{:S(2)}) collective-permute-start(bf16[2048,256]{1,0:T(8,128)(2,1)S(1)} %collective-permute-done.3.rest_4_), channel_id=1, source_target_pairs={{0,1},{1,0},{2,3},{3,2},{4,5},{5,4},{6,7},{7,6},{8,9},{9,8},{10,11... | collective-permute-start | bytes 3145736 | tf_op jit(solution)/shard_map/ppermute | solution.py:263
  62.1 16.8 %copy-start.12 = (bf16[128,2048]{1,0:T(8,128)(2,1)}, bf16[128,2048]{1,0:T(8,128)(2,1)S(1)}, u32[]{:S(2)}) copy-start(bf16[128,2048]{1,0:T(8,128)(2,1)S(1)} %collective-permute-done.11.rest_13_) | copy-start | bytes 1572868
  62.1 14.0 %collective-permute-start.6 = (bf16[1024,256]{1,0:T(8,128)(2,1)S(1)}, bf16[1024,256]{1,0:T(8,128)(2,1)S(1)}, u32[]{:S(2)}, u32[]{:S(2)}) collective-permute-start(bf16[1024,256]{1,0:T(8,128)(2,1)S(1)} %slice.17), channel_id=1, source_target_pairs={{0,6},{1,7},{2,0},{3,1},{4,2},{5,3},{6,4},{7,5},{8,14},{9,15},{10,... | collective-permute-start | bytes 1572872 | tf_op jit(solution)/shard_map/ppermute | solution.py:263
  64.7 14.1 %copy-start.13 = (bf16[128,2048]{1,0:T(8,128)(2,1)}, bf16[128,2048]{1,0:T(8,128)(2,1)S(1)}, u32[]{:S(2)}) copy-start(bf16[128,2048]{1,0:T(8,128)(2,1)S(1)} %collective-permute-done.13.rest_15_) | copy-start | bytes 1572868
  64.7 12.1 %collective-permute-start.16 = (bf16[64,2048]{1,0:T(8,128)(2,1)S(1)}, bf16[64,2048]{1,0:T(8,128)(2,1)S(1)}, u32[]{:S(2)}, u32[]{:S(2)}) collective-permute-start(bf16[64,2048]{1,0:T(8,128)(2,1)S(1)} %collective-permute-done.14.rest_16_), channel_id=1, source_target_pairs={{0,1},{1,0},{2,3},{3,2},{4,5},{5,4},{6,7},{7,6},{8,9},{9,8},{10,11... | collective-permute-start | bytes 786440 | tf_op jit(solution)/shard_map/ppermute | solution.py:263
  74.1 4.8 %copy-start.14 = (bf16[1024,256]{1,0:T(8,128)(2,1)}, bf16[1024,256]{1,0:T(8,128)(2,1)S(1)}, u32[]{:S(2)}) copy-start(bf16[1024,256]{1,0:T(8,128)(2,1)S(1)} %collective-permute-done.5.rest_6_) | copy-start | bytes 1572868
  74.1 4.7 %collective-permute-start.7 = (bf16[1024,256]{1,0:T(8,128)(2,1)S(1)}, bf16[1024,256]{1,0:T(8,128)(2,1)S(1)}, u32[]{:S(2)}, u32[]{:S(2)}) collective-permute-start(bf16[1024,256]{1,0:T(8,128)(2,1)S(1)} %collective-permute-done.5.rest_6_), channel_id=1, source_target_pairs={{0,1},{1,0},{2,3},{3,2},{4,5},{5,4},{6,7},{7,6},{8,9},{9,8},{10,11... | collective-permute-start | bytes 1572872 | tf_op jit(solution)/shard_map/ppermute | solution.py:263
  76.0 2.9 %copy-start.15 = (bf16[1024,256]{1,0:T(8,128)(2,1)}, bf16[1024,256]{1,0:T(8,128)(2,1)S(1)}, u32[]{:S(2)}) copy-start(bf16[1024,256]{1,0:T(8,128)(2,1)S(1)} %collective-permute-done.6.rest_7_) | copy-start | bytes 1572868
  76.0 5.0 %collective-permute-start.8 = (bf16[1024,256]{1,0:T(8,128)(2,1)S(1)}, bf16[1024,256]{1,0:T(8,128)(2,1)}, u32[]{:S(2)}, u32[]{:S(2)}) collective-permute-start(bf16[1024,256]{1,0:T(8,128)(2,1)S(1)} %collective-permute-done.6.rest_7_), channel_id=1, source_target_pairs={{0,1},{1,0},{2,3},{3,2},{4,5},{5,4},{6,7},{7,6},{8,9},{9,8},{10,11... | collective-permute-start | bytes 1572872 | tf_op jit(solution)/shard_map/ppermute | solution.py:263
  76.9 2.0 %copy-start.19 = (bf16[64,2048]{1,0:T(8,128)(2,1)}, bf16[64,2048]{1,0:T(8,128)(2,1)S(1)}, u32[]{:S(2)}) copy-start(bf16[64,2048]{1,0:T(8,128)(2,1)S(1)} %collective-permute-done.16.rest_18_) | copy-start | bytes 786436
  76.9 1.9 collective-permute-start.17
  78.8 0.7 copy-start.20
  78.8 1.1 copy-start.9
  78.8 1.4 copy-start.10
  80.2 0.8 copy-start.16
  100.2 6.7 %copy-start.7 = (f32[256]{0:T(256)S(1)}, f32[256]{0:T(256)}, u32[]{:S(2)}) copy-start(f32[256]{0:T(256)} %param.15) | copy-start | bytes 3076
  100.2 69.4 %all-to-all-start.1 = ((bf16[16,64,2048]{2,1,0:T(8,128)(2,1)}), bf16[16,64,2048]{2,1,0:T(8,128)(2,1)}, u32[]{:S(2)}, u32[]{:S(2)}) async-start(bf16[16,64,2048]{2,1,0:T(8,128)(2,1)} %bitcast.13), calls=%async_computation.1 | async-start | bytes 8388608 | tf_op jit(solution)/shard_map/all_to_all | solution.py:300

commit v3 on v2

--- a/solution.py
+++ b/solution.py
@@ -80,7 +80,7 @@
     )(rank, tokens, ids, gain)
 
 
-def expert_kernel(rows_hbm, *rest, gu_parts, dn_parts):
+def expert_kernel(rows_hbm, early_hbm, *rest, gu_parts, dn_parts):
     gu = rest[: len(gu_parts)]
     dn = rest[len(gu_parts) : len(gu_parts) + len(dn_parts)]
     out_hbm, rows_v, gu_v, dn_v, act_v, out_v, row_sem, gu_sem, dn_sem, out_sem = rest[len(gu_parts) + len(dn_parts) :]
@@ -138,7 +138,7 @@
         c.wait()
 
 
-def expert_unit(rows, gu, dn, parts, hid):
+def expert_unit(rows, early, gu, dn, parts, hid):
     total, width = rows.shape
     hbm = pl.BlockSpec(memory_space=pl.ANY)
     return pl.pallas_call(
@@ -148,7 +148,7 @@
             dn_parts=tuple((i, at, x.shape[0]) for i, at, x in dn),
         ),
         out_shape=jax.ShapeDtypeStruct((total, width), bf16),
-        in_specs=[hbm] * (1 + len(gu) + len(dn)),
+        in_specs=[hbm] * (2 + len(gu) + len(dn)),
         out_specs=hbm,
         scratch_shapes=[
             pltpu.VMEM((total, width), bf16),
@@ -166,7 +166,7 @@
             flops=6 * total * width * parts * hid, bytes_accessed=20 * 2**20, transcendentals=total * parts * hid
         ),
         name="expert_unit",
-    )(rows, *[x for _, _, x in gu], *[x for _, _, x in dn])
+    )(rows, early, *[x for _, _, x in gu], *[x for _, _, x in dn])
 
 
 def combine_kernel(rank, ids_ref, gates_ref, gain_ref, *rest, experts, split):
@@ -228,7 +228,8 @@
     slices, _, w = out_ref.shape
     for i in range(slices):
         span = pl.ds(i * w, w)
-        out_ref[i] = (acc_v[:, span] * scale * gain_ref[:, span]).astype(bf16)
+        gain = gain_ref[pl.ds(rank[0] ^ i, 1), :]
+        out_ref[i] = (acc_v[:, span] * scale * gain).astype(bf16)
 
 
 def combine(rank, ids, gates, gain, backs, rows, experts, split, slices):
@@ -243,7 +244,7 @@
             in_specs=[
                 pl.BlockSpec((top, rows), lambda s, r: (0, r[0])),
                 pl.BlockSpec((top, rows), lambda s, r: (0, r[0])),
-                pl.BlockSpec((1, width), lambda s, r: (0, 0)),
+                pl.BlockSpec(gain.shape, lambda s, r: (0, 0)),
             ]
             + [pl.BlockSpec(memory_space=pl.ANY)] * len(split),
             out_specs=pl.BlockSpec((slices, rows, width // slices), lambda s, r: (0, 0, 0)),
@@ -290,19 +291,22 @@
     gu = spread_out(gu_own)
     dn = spread_out(dn_own)
 
-    gain_full = lax.all_gather(out_gain, "tp", axis=0, tiled=True)
+    gains = [out_gain.reshape(1, -1)]
+    for d in range(1, n_tp):
+        gains.append(moved(gains[0], lambda i: i ^ d))
+    gain_near = jnp.concatenate(gains, axis=0)
     split = SPLIT(cap)
     outgoing = dispatch(rank, tokens, ids, norm_gain.reshape(1, width), experts, split)
     backs = []
     for x in outgoing:
         arrived = lax.all_to_all(x, "ep", split_axis=0, concat_axis=0, tiled=True)
-        result = expert_unit(arrived.reshape(-1, width), gu, dn, n_tp, down_weight.shape[1])
+        result = expert_unit(arrived.reshape(-1, width), gain_near, gu, dn, n_tp, down_weight.shape[1])
         back = lax.all_to_all(
             result.reshape(x.shape), "ep", split_axis=0, concat_axis=0, tiled=True
         )
         backs.append(back.reshape(-1, width))
     mixed = combine(
-        rank, ids, gates, gain_full.reshape(1, width), backs, rows, experts, split, n_tp,
+        rank, ids, gates, gain_near, backs, rows, experts, split, n_tp,
     )
     final = lax.all_to_all(mixed, "tp", split_axis=0, concat_axis=0, tiled=True)
     return final.reshape(n_tp * rows, width // n_tp)

time: 192 us -> 189 us (0.984)
  the two profiles are of different devices: /device:TPU:1 before, /device:TPU:2 now
where the time goes in v3:
time: 189 us; the launch traced here: 187 us
  blocking collectives  73 us (39%)
  waiting for transfers between devices  50 us (26%)
  starting transfers between devices  32.6 us (17%)
  Pallas kernels  28.8 us (15%)
  local copies, waits for them, and re-layouts  2.27 us (1%)
    all_to_all x1, blocking collectives, local(): lax.all_to_all(result.reshape(x.shape), 'ep', split_axis=0, concat_axis=0...  57.5 us
    ppermute x25, waiting for transfers between devices, moved(): return lax.ppermute(x, 'tp', [(i, step(i)) for i in range(n)])  50 us
    ppermute x25, starting transfers between devices, moved(): return lax.ppermute(x, 'tp', [(i, step(i)) for i in range(n)])  24.1 us
    pallas_call x1, Pallas kernels, expert_unit(): pl.pallas_call(functools.partial(expert_kernel, gu_parts=tuple(((i, at, x...  19.2 us
    all_to_all x1, blocking collectives, local(): final = lax.all_to_all(mixed, 'tp', split_axis=0, concat_axis=0, tiled=True)  15.4 us
    all_to_all x1, starting transfers between devices, local(): arrived = lax.all_to_all(x, 'ep', split_axis=0, concat_axis=0, tiled=True)  8.46 us
    pallas_call x1, Pallas kernels, combine(): pl.pallas_call(functools.partial(combine_kernel, experts=experts, split=s...  4.93 us
    pallas_call x1, Pallas kernels, dispatch(): pl.pallas_call(functools.partial(dispatch_kernel, experts=experts, cap=su...  4.66 us
  transfers between devices with their start and end apart: 26, of which 7 were waited for; matrix products, arithmetic and copies ran while one was open for 0% of the time, Pallas kernels for 0%

profile of v3, /device:TPU:2, one launch (start us, length us, event | category | flops | bytes accessed | tf_op | source)
XLA Modules:
  0.0 187.0 jit_solution(13620362928466425304)
XLA Ops:
  0.0 4.7 %dispatch.1 = bf16[16,64,2048]{2,1,0:T(8,128)(2,1)} custom-call(s32[1]{0:T(128)} %bitcast.rank, bf16[128,2048]{1,0:T(8,128)(2,1)} %tokens_ref.1, s32[4,1024]{1,0:T(4,128)} %bitcast.17, f32[1,2048]{1,0:T(1,128)} %bitcast.20), custom_call_target="tpu_custom_call" | custom-call | tf_op jit(solution)/shard_map/dispatch/pallas_call | solution.py:62
  4.7 8.5 %all-to-all-start = ((bf16[16,64,2048]{2,1,0:T(8,128)(2,1)}), bf16[16,64,2048]{2,1,0:T(8,128)(2,1)}, u32[]{:S(2)}, u32[]{:S(2)}) async-start(bf16[16,64,2048]{2,1,0:T(8,128)(2,1)} %dispatch.1), calls=%async_computation | async-start | bytes 8388608 | tf_op jit(solution)/shard_map/all_to_all | solution.py:302
  13.1 0.0 copy-done.1
  13.1 0.1 pad_maximum_fusion.rest_0_
  13.3 1.6 collective-permute-start.8
  14.9 1.7 collective-permute-start.10
  16.6 0.0 copy-done.7
  16.6 0.0 collective-permute-start
  16.6 0.4 collective-permute-start.1
  16.9 1.5 collective-permute-start.2
  18.4 0.0 collective-permute-done
  18.5 2.0 %collective-permute-start.3 = (f32[1,256]{1,0:T(1,128)S(1)}, f32[1,256]{1,0:T(1,128)S(1)}, u32[]{:S(2)}, u32[]{:S(2)}) collective-permute-start(f32[1,256]{1,0:T(1,128)S(1)} %bitcast.24), channel_id=1, source_target_pairs={{0,4},{1,5},{2,6},{3,7},{4,0},{5,1},{6,2},{7,3},{8,12},{9,13},{10,... | collective-permute-start | bytes 3080 | tf_op jit(solution)/shard_map/ppermute | solution.py:264
  20.4 18.6 %collective-permute-done.1 = f32[1,256]{1,0:T(1,128)S(1)} collective-permute-done((f32[1,256]{1,0:T(1,128)S(1)}, f32[1,256]{1,0:T(1,128)S(1)}, u32[]{:S(2)}, u32[]{:S(2)}) %collective-permute-start.1) | collective-permute-done | bytes 1056 | tf_op jit(solution)/shard_map/ppermute | solution.py:264
  39.1 0.7 collective-permute-start.4
  39.8 0.0 collective-permute-done.2
  39.8 1.0 collective-permute-start.5
  40.8 0.0 collective-permute-done.3
  40.8 3.9 %collective-permute-start.6 = (f32[1,256]{1,0:T(1,128)S(1)}, f32[1,256]{1,0:T(1,128)S(1)}, u32[]{:S(2)}, u32[]{:S(2)}) collective-permute-start(f32[1,256]{1,0:T(1,128)S(1)} %bitcast.27), channel_id=1, source_target_pairs={{0,7},{1,6},{2,5},{3,4},{4,3},{5,2},{6,1},{7,0},{8,15},{9,14},{10,... | collective-permute-start | bytes 3080 | tf_op jit(solution)/shard_map/ppermute | solution.py:264
  44.6 0.0 collective-permute-done.4
  44.7 0.0 collective-permute-start.17
  44.7 0.0 collective-permute-done.5
  44.7 1.5 collective-permute-start.7
  46.1 0.0 collective-permute-done.6
  46.1 1.8 collective-permute-start.19
  48.0 11.0 %collective-permute-done.17.rest_12_ = bf16[128,2048]{1,0:T(8,128)(2,1)S(1)} collective-permute-done((bf16[128,2048]{1,0:T(8,128)(2,1)}, bf16[128,2048]{1,0:T(8,128)(2,1)S(1)}, u32[]{:S(2)}, u32[]{:S(2)}) %collective-permute-start.17) | collective-permute-done | bytes 524320 | tf_op jit(solution)/shard_map/ppermute | solution.py:264
  59.0 0.0 collective-permute-start.16
  59.0 1.8 collective-permute-done.19.rest_14_
  60.8 0.0 collective-permute-start.18
  60.9 0.0 collective-permute-done.8.rest_2_
  60.9 0.2 collective-permute-start.21
  61.1 0.0 collective-permute-done.10.rest_4_
  61.1 3.5 %collective-permute-start.22 = (bf16[64,2048]{1,0:T(8,128)(2,1)S(1)}, bf16[64,2048]{1,0:T(8,128)(2,1)}, u32[]{:S(2)}, u32[]{:S(2)}) collective-permute-start(bf16[64,2048]{1,0:T(8,128)(2,1)S(1)} %slice.19), channel_id=1, source_target_pairs={{0,6},{1,7},{2,0},{3,1},{4,2},{5,3},{6,4},{7,5},{8,14},{9,15},{10,... | collective-permute-start | bytes 786440 | tf_op jit(solution)/shard_map/ppermute | solution.py:264
  64.7 0.0 collective-permute-done.16.rest_11_
  64.7 0.0 copy-start.9
  64.8 0.1 collective-permute-start.20
  64.9 6.2 %collective-permute-done.21.rest_16_ = bf16[64,2048]{1,0:T(8,128)(2,1)S(1)} collective-permute-done((bf16[64,2048]{1,0:T(8,128)(2,1)S(1)}, bf16[64,2048]{1,0:T(8,128)(2,1)S(1)}, u32[]{:S(2)}, u32[]{:S(2)}) %collective-permute-start.21) | collective-permute-done | bytes 262176 | tf_op jit(solution)/shard_map/ppermute | solution.py:264
  71.0 0.0 collective-permute-start.12
  71.0 0.0 collective-permute-done.22.rest_17_
  71.0 0.1 collective-permute-start.9
  71.1 0.0 collective-permute-done.7.rest_1_
  71.2 0.5 collective-permute-start.11
  71.6 0.0 collective-permute-done.18.rest_13_
  71.6 3.2 %collective-permute-start.13 = (bf16[1024,256]{1,0:T(8,128)(2,1)S(1)}, bf16[1024,256]{1,0:T(8,128)(2,1)}, u32[]{:S(2)}, u32[]{:S(2)}) collective-permute-start(bf16[1024,256]{1,0:T(8,128)(2,1)S(1)} %slice.17), channel_id=1, source_target_pairs={{0,6},{1,7},{2,0},{3,1},{4,2},{5,3},{6,4},{7,5},{8,14},{9,15},{10,... | collective-permute-start | bytes 1572872 | tf_op jit(solution)/shard_map/ppermute | solution.py:264
  74.8 0.0 collective-permute-done.20.rest_15_
  74.8 0.0 collective-permute-start.23
  74.8 10.8 %collective-permute-done.12.rest_6_ = bf16[1024,256]{1,0:T(8,128)(2,1)} collective-permute-done((bf16[1024,256]{1,0:T(8,128)(2,1)S(1)}, bf16[1024,256]{1,0:T(8,128)(2,1)}, u32[]{:S(2)}, u32[]{:S(2)}) %collective-permute-start.12) | collective-permute-done | bytes 524320 | tf_op jit(solution)/shard_map/ppermute | solution.py:264
  85.6 0.0 collective-permute-start.14
  85.6 0.6 collective-permute-done.13.rest_7_
  86.2 0.0 collective-permute-start.15
  86.2 0.0 collective-permute-done.23.rest_18_
  86.3 0.7 copy-done.13
  87.0 0.5 collective-permute-start.24
  87.5 0.6 concatenate.6.early_hbm.gain_ref
  88.1 0.9 collective-permute-done.24.rest_19_
  89.0 0.0 collective-permute-done.9.rest_3_
  89.0 0.0 collective-permute-done.11.rest_5_
  89.0 0.0 collective-permute-done.14.rest_8_
  89.0 0.0 collective-permute-done.15.rest_9_
  89.0 0.0 all-to-all-done
  89.1 19.2 %expert_unit.1 = bf16[1024,2048]{1,0:T(8,128)(2,1)} custom-call(bf16[1024,2048]{1,0:T(8,128)(2,1)} %bitcast.5.rows_hbm, f32[8,256]{1,0:T(8,128)} %concatenate.6.early_hbm.gain_ref, bf16[2048,256]{1,0:T(8,128)(2,1)} %copy-done, bf16[2048,256]{1,0:T(8,128)(2,1)} %copy-done.8, bf16[2048,256]{1,0:T(8,128)(2,1)} %copy-done.3, ...), custom_call_target="tpu_custom_call" | custom-call | flops 12884901888 | bytes 20971520 | tf_op jit(solution)/shard_map/expert_unit/pallas_call | solution.py:144
  108.3 57.5 %all_to_all.15 = bf16[16,64,2048]{2,1,0:T(8,128)(2,1)} all-to-all(bf16[16,64,2048]{2,1,0:T(8,128)(2,1)} %bitcast.13), channel_id=1, replica_groups=mesh['ep'=16,'tp'=8] {'ep'}, dimensions={0} | all-to-all | bytes 8388608 | tf_op jit(solution)/shard_map/all_to_all | solution.py:304
  165.8 4.9 %combine.1 = bf16[8,128,256]{2,1,0:T(8,128)(2,1)} custom-call(s32[1]{0:T(128)} %bitcast.rank, s32[4,1024]{1,0:T(4,128)} %bitcast.18, f32[4,1024]{1,0:T(4,128)} %bitcast.19, f32[8,256]{1,0:T(8,128)} %concatenate.6.early_hbm.gain_ref, bf16[1024,2048]{1,0:T(8,128)(2,1)} %bitcast.12), custom_call_target="tpu_custom_call" | custom-call | tf_op jit(solution)/shard_map/combine/pallas_call | solution.py:238
  170.7 15.4 %all_to_all.16 = bf16[8,128,256]{2,1,0:T(8,128)(2,1)S(1)} all-to-all(bf16[8,128,256]{2,1,0:T(8,128)(2,1)} %combine.1), channel_id=1, replica_groups=mesh['ep'=16,'tp'=8] {'tp'}, dimensions={0} | all-to-all | bytes 1048576 | tf_op jit(solution)/shard_map/all_to_all | solution.py:311
  186.2 0.8 copy.10
  (28 shorter events, 0.2 us)
Async XLA Ops:
  4.7 8.5 %copy-start.1 = (bf16[1,2048,128]{2,1,0:T(8,128)(2,1)S(1)}, bf16[1,2048,128]{2,1,0:T(8,128)(2,1)}, u32[]{:S(2)}) copy-start(bf16[1,2048,128]{2,1,0:T(8,128)(2,1)} %param.13) | copy-start | bytes 1572868
  4.7 8.5 %copy-start.2 = (bf16[1,2048,128]{2,1,0:T(8,128)(2,1)S(1)}, bf16[1,2048,128]{2,1,0:T(8,128)(2,1)}, u32[]{:S(2)}) copy-start(bf16[1,2048,128]{2,1,0:T(8,128)(2,1)} %param.12) | copy-start | bytes 1572868
  4.7 11.9 %copy-start.7 = (f32[256]{0:T(256)S(1)}, f32[256]{0:T(256)}, u32[]{:S(2)}) copy-start(f32[256]{0:T(256)} %param.15) | copy-start | bytes 3076
  4.7 84.4 %all-to-all-start = ((bf16[16,64,2048]{2,1,0:T(8,128)(2,1)}), bf16[16,64,2048]{2,1,0:T(8,128)(2,1)}, u32[]{:S(2)}, u32[]{:S(2)}) async-start(bf16[16,64,2048]{2,1,0:T(8,128)(2,1)} %dispatch.1), calls=%async_computation | async-start | bytes 8388608 | tf_op jit(solution)/shard_map/all_to_all | solution.py:302
  13.3 75.8 %copy-start = (bf16[2048,256]{1,0:T(8,128)(2,1)}, bf16[2048,256]{1,0:T(8,128)(2,1)S(1)}, u32[]{:S(2)}) copy-start(bf16[2048,256]{1,0:T(8,128)(2,1)S(1)} %pad_maximum_fusion.rest_0_) | copy-start | bytes 3145732
  13.3 47.6 %collective-permute-start.8 = (bf16[2048,256]{1,0:T(8,128)(2,1)S(1)}, bf16[2048,256]{1,0:T(8,128)(2,1)S(1)}, u32[]{:S(2)}, u32[]{:S(2)}) collective-permute-start(bf16[2048,256]{1,0:T(8,128)(2,1)S(1)} %pad_maximum_fusion.rest_0_), channel_id=1, source_target_pairs={{0,2},{1,3},{2,4},{3,5},{4,6},{5,7},{6,0},{7,1},{8,10},{9,11},{10,... | collective-permute-start | bytes 3145736 | tf_op jit(solution)/shard_map/ppermute | solution.py:264
  14.9 46.2 %collective-permute-start.10 = (bf16[2048,256]{1,0:T(8,128)(2,1)S(1)}, bf16[2048,256]{1,0:T(8,128)(2,1)S(1)}, u32[]{:S(2)}, u32[]{:S(2)}) collective-permute-start(bf16[2048,256]{1,0:T(8,128)(2,1)S(1)} %pad_maximum_fusion.rest_0_), channel_id=1, source_target_pairs={{0,6},{1,7},{2,0},{3,1},{4,2},{5,3},{6,4},{7,5},{8,14},{9,15},{10,... | collective-permute-start | bytes 3145736 | tf_op jit(solution)/shard_map/ppermute | solution.py:264
  16.6 1.9 collective-permute-start
  16.6 22.5 %collective-permute-start.1 = (f32[1,256]{1,0:T(1,128)S(1)}, f32[1,256]{1,0:T(1,128)S(1)}, u32[]{:S(2)}, u32[]{:S(2)}) collective-permute-start(f32[1,256]{1,0:T(1,128)S(1)} %bitcast.22), channel_id=1, source_target_pairs={{0,2},{1,3},{2,0},{3,1},{4,6},{5,7},{6,4},{7,5},{8,10},{9,11},{10,... | collective-permute-start | bytes 3080 | tf_op jit(solution)/shard_map/ppermute | solution.py:264
  16.9 22.8 %collective-permute-start.2 = (f32[1,256]{1,0:T(1,128)S(1)}, f32[1,256]{1,0:T(1,128)S(1)}, u32[]{:S(2)}, u32[]{:S(2)}) collective-permute-start(f32[1,256]{1,0:T(1,128)S(1)} %bitcast.23), channel_id=1, source_target_pairs={{0,3},{1,2},{2,1},{3,0},{4,7},{5,6},{6,5},{7,4},{8,11},{9,10},{10,... | collective-permute-start | bytes 3080 | tf_op jit(solution)/shard_map/ppermute | solution.py:264
  18.5 22.3 %collective-permute-start.3 = (f32[1,256]{1,0:T(1,128)S(1)}, f32[1,256]{1,0:T(1,128)S(1)}, u32[]{:S(2)}, u32[]{:S(2)}) collective-permute-start(f32[1,256]{1,0:T(1,128)S(1)} %bitcast.24), channel_id=1, source_target_pairs={{0,4},{1,5},{2,6},{3,7},{4,0},{5,1},{6,2},{7,3},{8,12},{9,13},{10,... | collective-permute-start | bytes 3080 | tf_op jit(solution)/shard_map/ppermute | solution.py:264
  39.1 5.6 %collective-permute-start.4 = (f32[1,256]{1,0:T(1,128)S(1)}, f32[1,256]{1,0:T(1,128)S(1)}, u32[]{:S(2)}, u32[]{:S(2)}) collective-permute-start(f32[1,256]{1,0:T(1,128)S(1)} %bitcast.25), channel_id=1, source_target_pairs={{0,5},{1,4},{2,7},{3,6},{4,1},{5,0},{6,3},{7,2},{8,13},{9,12},{10,... | collective-permute-start | bytes 3080 | tf_op jit(solution)/shard_map/ppermute | solution.py:264
  39.8 4.9 %collective-permute-start.5 = (f32[1,256]{1,0:T(1,128)S(1)}, f32[1,256]{1,0:T(1,128)S(1)}, u32[]{:S(2)}, u32[]{:S(2)}) collective-permute-start(f32[1,256]{1,0:T(1,128)S(1)} %bitcast.26), channel_id=1, source_target_pairs={{0,6},{1,7},{2,4},{3,5},{4,2},{5,3},{6,0},{7,1},{8,14},{9,15},{10,... | collective-permute-start | bytes 3080 | tf_op jit(solution)/shard_map/ppermute | solution.py:264
  40.8 5.3 %collective-permute-start.6 = (f32[1,256]{1,0:T(1,128)S(1)}, f32[1,256]{1,0:T(1,128)S(1)}, u32[]{:S(2)}, u32[]{:S(2)}) collective-permute-start(f32[1,256]{1,0:T(1,128)S(1)} %bitcast.27), channel_id=1, source_target_pairs={{0,7},{1,6},{2,5},{3,4},{4,3},{5,2},{6,1},{7,0},{8,15},{9,14},{10,... | collective-permute-start | bytes 3080 | tf_op jit(solution)/shard_map/ppermute | solution.py:264
  44.7 14.3 %collective-permute-start.17 = (bf16[128,2048]{1,0:T(8,128)(2,1)}, bf16[128,2048]{1,0:T(8,128)(2,1)S(1)}, u32[]{:S(2)}, u32[]{:S(2)}) collective-permute-start(bf16[128,2048]{1,0:T(8,128)(2,1)} %bitcast.29), channel_id=1, source_target_pairs={{0,2},{1,3},{2,4},{3,5},{4,6},{5,7},{6,0},{7,1},{8,10},{9,11},{10,... | collective-permute-start | bytes 1572872 | tf_op jit(solution)/shard_map/ppermute | solution.py:264
  44.7 26.5 %collective-permute-start.7 = (bf16[2048,256]{1,0:T(8,128)(2,1)S(1)}, bf16[2048,256]{1,0:T(8,128)(2,1)S(1)}, u32[]{:S(2)}, u32[]{:S(2)}) collective-permute-start(bf16[2048,256]{1,0:T(8,128)(2,1)S(1)} %pad_maximum_fusion.rest_0_), channel_id=1, source_target_pairs={{0,1},{1,0},{2,3},{3,2},{4,5},{5,4},{6,7},{7,6},{8,9},{9,8},{10,11... | collective-permute-start | bytes 3145736 | tf_op jit(solution)/shard_map/ppermute | solution.py:264
  46.1 14.7 %collective-permute-start.19 = (bf16[128,2048]{1,0:T(8,128)(2,1)}, bf16[128,2048]{1,0:T(8,128)(2,1)S(1)}, u32[]{:S(2)}, u32[]{:S(2)}) collective-permute-start(bf16[128,2048]{1,0:T(8,128)(2,1)} %bitcast.30), channel_id=1, source_target_pairs={{0,6},{1,7},{2,0},{3,1},{4,2},{5,3},{6,4},{7,5},{8,14},{9,15},{10,... | collective-permute-start | bytes 1572872 | tf_op jit(solution)/shard_map/ppermute | solution.py:264
  59.0 27.2 %copy-start.5 = (bf16[128,2048]{1,0:T(8,128)(2,1)}, bf16[128,2048]{1,0:T(8,128)(2,1)S(1)}, u32[]{:S(2)}) copy-start(bf16[128,2048]{1,0:T(8,128)(2,1)S(1)} %collective-permute-done.17.rest_12_) | copy-start | bytes 1572868
  59.0 5.8 %collective-permute-start.16 = (bf16[128,2048]{1,0:T(8,128)(2,1)}, bf16[128,2048]{1,0:T(8,128)(2,1)S(1)}, u32[]{:S(2)}, u32[]{:S(2)}) collective-permute-start(bf16[128,2048]{1,0:T(8,128)(2,1)} %bitcast.31), channel_id=1, source_target_pairs={{0,1},{1,0},{2,3},{3,2},{4,5},{5,4},{6,7},{7,6},{8,9},{9,8},{10,11... | collective-permute-start | bytes 1572872 | tf_op jit(solution)/shard_map/ppermute | solution.py:264
  60.8 25.4 %copy-start.6 = (bf16[128,2048]{1,0:T(8,128)(2,1)}, bf16[128,2048]{1,0:T(8,128)(2,1)S(1)}, u32[]{:S(2)}) copy-start(bf16[128,2048]{1,0:T(8,128)(2,1)S(1)} %collective-permute-done.19.rest_14_) | copy-start | bytes 1572868
  60.8 10.8 %collective-permute-start.18 = (bf16[128,2048]{1,0:T(8,128)(2,1)S(1)}, bf16[128,2048]{1,0:T(8,128)(2,1)S(1)}, u32[]{:S(2)}, u32[]{:S(2)}) collective-permute-start(bf16[128,2048]{1,0:T(8,128)(2,1)S(1)} %collective-permute-done.17.rest_12_), channel_id=1, source_target_pairs={{0,1},{1,0},{2,3},{3,2},{4,5},{5,4},{6,7},{7,6},{8,9},{9,8},{10,11... | collective-permute-start | bytes 1572872 | tf_op jit(solution)/shard_map/ppermute | solution.py:264
  60.9 28.2 %copy-start.3 = (bf16[2048,256]{1,0:T(8,128)(2,1)}, bf16[2048,256]{1,0:T(8,128)(2,1)S(1)}, u32[]{:S(2)}) copy-start(bf16[2048,256]{1,0:T(8,128)(2,1)S(1)} %collective-permute-done.8.rest_2_) | copy-start | bytes 3145732
  60.9 10.1 %collective-permute-start.21 = (bf16[64,2048]{1,0:T(8,128)(2,1)S(1)}, bf16[64,2048]{1,0:T(8,128)(2,1)S(1)}, u32[]{:S(2)}, u32[]{:S(2)}) collective-permute-start(bf16[64,2048]{1,0:T(8,128)(2,1)S(1)} %slice.18), channel_id=1, source_target_pairs={{0,2},{1,3},{2,4},{3,5},{4,6},{5,7},{6,0},{7,1},{8,10},{9,11},{10,... | collective-permute-start | bytes 786440 | tf_op jit(solution)/shard_map/ppermute | solution.py:264
  61.1 27.9 %copy-start.4 = (bf16[2048,256]{1,0:T(8,128)(2,1)}, bf16[2048,256]{1,0:T(8,128)(2,1)S(1)}, u32[]{:S(2)}) copy-start(bf16[2048,256]{1,0:T(8,128)(2,1)S(1)} %collective-permute-done.10.rest_4_) | copy-start | bytes 3145732
  61.1 9.9 %collective-permute-start.22 = (bf16[64,2048]{1,0:T(8,128)(2,1)S(1)}, bf16[64,2048]{1,0:T(8,128)(2,1)}, u32[]{:S(2)}, u32[]{:S(2)}) collective-permute-start(bf16[64,2048]{1,0:T(8,128)(2,1)S(1)} %slice.19), channel_id=1, source_target_pairs={{0,6},{1,7},{2,0},{3,1},{4,2},{5,3},{6,4},{7,5},{8,14},{9,15},{10,... | collective-permute-start | bytes 786440 | tf_op jit(solution)/shard_map/ppermute | solution.py:264
  64.7 21.5 %copy-start.9 = (bf16[128,2048]{1,0:T(8,128)(2,1)}, bf16[128,2048]{1,0:T(8,128)(2,1)S(1)}, u32[]{:S(2)}) copy-start(bf16[128,2048]{1,0:T(8,128)(2,1)S(1)} %collective-permute-done.16.rest_11_) | copy-start | bytes 1572868
  64.8 10.0 %collective-permute-start.20 = (bf16[128,2048]{1,0:T(8,128)(2,1)S(1)}, bf16[128,2048]{1,0:T(8,128)(2,1)S(1)}, u32[]{:S(2)}, u32[]{:S(2)}) collective-permute-start(bf16[128,2048]{1,0:T(8,128)(2,1)S(1)} %collective-permute-done.19.rest_14_), channel_id=1, source_target_pairs={{0,1},{1,0},{2,3},{3,2},{4,5},{5,4},{6,7},{7,6},{8,9},{9,8},{10,11... | collective-permute-start | bytes 1572872 | tf_op jit(solution)/shard_map/ppermute | solution.py:264
  71.0 18.0 %copy-start.12 = (bf16[64,2048]{1,0:T(8,128)(2,1)}, bf16[64,2048]{1,0:T(8,128)(2,1)S(1)}, u32[]{:S(2)}) copy-start(bf16[64,2048]{1,0:T(8,128)(2,1)S(1)} %collective-permute-done.21.rest_16_) | copy-start | bytes 786436
  71.0 14.6 %collective-permute-start.12 = (bf16[1024,256]{1,0:T(8,128)(2,1)S(1)}, bf16[1024,256]{1,0:T(8,128)(2,1)}, u32[]{:S(2)}, u32[]{:S(2)}) collective-permute-start(bf16[1024,256]{1,0:T(8,128)(2,1)S(1)} %slice.16), channel_id=1, source_target_pairs={{0,2},{1,3},{2,4},{3,5},{4,6},{5,7},{6,0},{7,1},{8,10},{9,11},{10,... | collective-permute-start | bytes 1572872 | tf_op jit(solution)/shard_map/ppermute | solution.py:264
  71.0 18.0 %collective-permute-start.9 = (bf16[2048,256]{1,0:T(8,128)(2,1)S(1)}, bf16[2048,256]{1,0:T(8,128)(2,1)}, u32[]{:S(2)}, u32[]{:S(2)}) collective-permute-start(bf16[2048,256]{1,0:T(8,128)(2,1)S(1)} %collective-permute-done.8.rest_2_), channel_id=1, source_target_pairs={{0,1},{1,0},{2,3},{3,2},{4,5},{5,4},{6,7},{7,6},{8,9},{9,8},{10,11... | collective-permute-start | bytes 3145736 | tf_op jit(solution)/shard_map/ppermute | solution.py:264
  71.1 15.1 %copy-start.8 = (bf16[2048,256]{1,0:T(8,128)(2,1)}, bf16[2048,256]{1,0:T(8,128)(2,1)S(1)}, u32[]{:S(2)}) copy-start(bf16[2048,256]{1,0:T(8,128)(2,1)S(1)} %collective-permute-done.7.rest_1_) | copy-start | bytes 3145732
  71.2 17.9 %collective-permute-start.11 = (bf16[2048,256]{1,0:T(8,128)(2,1)S(1)}, bf16[2048,256]{1,0:T(8,128)(2,1)}, u32[]{:S(2)}, u32[]{:S(2)}) collective-permute-start(bf16[2048,256]{1,0:T(8,128)(2,1)S(1)} %collective-permute-done.10.rest_4_), channel_id=1, source_target_pairs={{0,1},{1,0},{2,3},{3,2},{4,5},{5,4},{6,7},{7,6},{8,9},{9,8},{10,11... | collective-permute-start | bytes 3145736 | tf_op jit(solution)/shard_map/ppermute | solution.py:264
  71.6 14.6 %copy-start.10 = (bf16[128,2048]{1,0:T(8,128)(2,1)}, bf16[128,2048]{1,0:T(8,128)(2,1)S(1)}, u32[]{:S(2)}) copy-start(bf16[128,2048]{1,0:T(8,128)(2,1)S(1)} %collective-permute-done.18.rest_13_) | copy-start | bytes 1572868
  71.6 14.6 %collective-permute-start.13 = (bf16[1024,256]{1,0:T(8,128)(2,1)S(1)}, bf16[1024,256]{1,0:T(8,128)(2,1)}, u32[]{:S(2)}, u32[]{:S(2)}) collective-permute-start(bf16[1024,256]{1,0:T(8,128)(2,1)S(1)} %slice.17), channel_id=1, source_target_pairs={{0,6},{1,7},{2,0},{3,1},{4,2},{5,3},{6,4},{7,5},{8,14},{9,15},{10,... | collective-permute-start | bytes 1572872 | tf_op jit(solution)/shard_map/ppermute | solution.py:264
  74.8 11.5 %copy-start.11 = (bf16[128,2048]{1,0:T(8,128)(2,1)}, bf16[128,2048]{1,0:T(8,128)(2,1)S(1)}, u32[]{:S(2)}) copy-start(bf16[128,2048]{1,0:T(8,128)(2,1)S(1)} %collective-permute-done.20.rest_15_) | copy-start | bytes 1572868
  74.8 11.4 %collective-permute-start.23 = (bf16[64,2048]{1,0:T(8,128)(2,1)S(1)}, bf16[64,2048]{1,0:T(8,128)(2,1)S(1)}, u32[]{:S(2)}, u32[]{:S(2)}) collective-permute-start(bf16[64,2048]{1,0:T(8,128)(2,1)S(1)} %collective-permute-done.21.rest_16_), channel_id=1, source_target_pairs={{0,1},{1,0},{2,3},{3,2},{4,5},{5,4},{6,7},{7,6},{8,9},{9,8},{10,11... | collective-permute-start | bytes 786440 | tf_op jit(solution)/shard_map/ppermute | solution.py:264
  85.6 3.4 %collective-permute-start.14 = (bf16[1024,256]{1,0:T(8,128)(2,1)}, bf16[1024,256]{1,0:T(8,128)(2,1)}, u32[]{:S(2)}, u32[]{:S(2)}) collective-permute-start(bf16[1024,256]{1,0:T(8,128)(2,1)} %collective-permute-done.12.rest_6_), channel_id=1, source_target_pairs={{0,1},{1,0},{2,3},{3,2},{4,5},{5,4},{6,7},{7,6},{8,9},{9,8},{10,11... | collective-permute-start | bytes 1572872 | tf_op jit(solution)/shard_map/ppermute | solution.py:264
  86.2 2.8 %collective-permute-start.15 = (bf16[1024,256]{1,0:T(8,128)(2,1)}, bf16[1024,256]{1,0:T(8,128)(2,1)}, u32[]{:S(2)}, u32[]{:S(2)}) collective-permute-start(bf16[1024,256]{1,0:T(8,128)(2,1)} %collective-permute-done.13.rest_7_), channel_id=1, source_target_pairs={{0,1},{1,0},{2,3},{3,2},{4,5},{5,4},{6,7},{7,6},{8,9},{9,8},{10,11... | collective-permute-start | bytes 1572872 | tf_op jit(solution)/shard_map/ppermute | solution.py:264
  86.3 0.7 copy-start.13
  87.0 2.0 %collective-permute-start.24 = (bf16[64,2048]{1,0:T(8,128)(2,1)}, bf16[64,2048]{1,0:T(8,128)(2,1)}, u32[]{:S(2)}, u32[]{:S(2)}) collective-permute-start(bf16[64,2048]{1,0:T(8,128)(2,1)} %collective-permute-done.22.rest_17_), channel_id=1, source_target_pairs={{0,1},{1,0},{2,3},{3,2},{4,5},{5,4},{6,7},{7,6},{8,9},{9,8},{10,11... | collective-permute-start | bytes 786440 | tf_op jit(solution)/shard_map/ppermute | solution.py:264
